TPU v7x, 128 devices: a whole 4x4x4 slice. The times are simulated.
128 devices in a mesh: ra: 16 (over z, y), cb: 8 (over x, core).
Axes of the slice: x: 4, y: 4, z: 4, core: 2. Of those that a mesh axis runs over, the one named last changes fastest.
Arguments:
- tokens: bfloat16 [1024, 4096], P(None, 'ra'), may hold values from -40 to 40
- norm_gain: float32 [4096], P('ra'), may hold values from 0.1 to 1.9
- gate_weight: bfloat16 [4096, 11264], P('ra', 'cb'), may hold values from -0.09375 to 0.09375
- up_weight: bfloat16 [4096, 11264], P('ra', 'cb'), may hold values from -0.09375 to 0.09375
- down_weight: bfloat16 [11264, 4096], P('cb', 'ra'), may hold values from -0.0546875 to 0.0546875
- out_gain: float32 [4096], P('ra'), may hold values from 0.1 to 1.9
Outputs:
- normed: bfloat16 [1024, 4096], P(None, 'ra')
All inputs are finite; a program needn't handle non-finite values.
Results may differ from a plain program's by a relative error of at most 0.0076.
Values may be sent and summed in bfloat16 or wider, within the bound.
A program may use at most 128 MiB of HBM per device.

v0:
```python
import jax
import jax.numpy as jnp
from jax import lax
from jax.sharding import PartitionSpec as P

D = 4096


def in_blocks(x, dim, length):
    before, after = (x.shape[:dim], x.shape[dim + 1 :])
    return jnp.moveaxis(x.reshape(*before, length, -1, *after), dim, 0)


def summed_on_arrival(x, axis, dim):
    length = lax.axis_size(axis)
    pieces = lax.all_to_all(in_blocks(x, dim, length), axis, 0, 0, tiled=True)
    return jnp.sum(pieces.astype(jnp.float32), axis=0)


def sent_together(arrays, axis, dim, along):
    columns = [a.reshape(*a.shape[:along], -1) for a in arrays]
    both = jnp.concatenate(columns, axis=along)
    out, at, finished = (summed_on_arrival(both, axis, dim), 0, [])
    for a, column in zip(arrays, columns):
        section = out[..., at : at + column.shape[along]]
        finished.append(section.reshape(*section.shape[:along], *a.shape[along:]))
        at += column.shape[along]
    return tuple(finished)


def copy_for_each(x, axis):
    length = lax.axis_size(axis)
    return lax.all_to_all(jnp.broadcast_to(x[None], (length, *x.shape)), axis, 0, 0, tiled=True)


def of_everyone(x, axis):
    everything = copy_for_each(x, axis)
    return jnp.sum(everything.astype(jnp.float32), axis=0)


def taken_together(x, axis):
    return copy_for_each(x, axis).sum(axis=0)


def body(tokens, norm_gain, gate_weight, up_weight, down_weight, out_gain):
    stream_in = tokens.astype(jnp.float32)
    local_sq = jnp.sum(stream_in * stream_in, axis=1)
    scaled = (stream_in * norm_gain[None, :]).astype(jnp.bfloat16)
    gate_part = jnp.dot(scaled, gate_weight, preferred_element_type=jnp.float32)
    up_part = jnp.dot(scaled, up_weight, preferred_element_type=jnp.float32)
    gate_sum, up_sum, sq_sum = sent_together(
        (
            gate_part.astype(jnp.bfloat16),
            up_part.astype(jnp.bfloat16),
            local_sq.astype(jnp.bfloat16),
        ),
        "ra",
        0,
        1,
    )
    inv_rms = jax.lax.rsqrt(sq_sum / D + 1e-06)[:, None]
    hidden = (jax.nn.silu(gate_sum * inv_rms) * (up_sum * inv_rms)).astype(jnp.bfloat16)
    down_part = jnp.dot(
        lax.all_gather(hidden, "ra", axis=0, tiled=True),
        down_weight,
        preferred_element_type=jnp.float32,
    )
    branch = of_everyone(down_part.astype(jnp.bfloat16), "cb").astype(jnp.float32)
    stream = 0.5 * stream_in + branch
    total_sq = taken_together(jnp.sum(stream * stream, axis=1), "ra")
    factor = jax.lax.rsqrt(total_sq / D + 1e-06)[:, None]
    return (stream * factor * out_gain[None, :]).astype(jnp.bfloat16)


def solution(mesh):
    placed = (P(None, "ra"), P("ra"), P("ra", "cb"), P("ra", "cb"), P("cb", "ra"), P("ra"))
    return jax.shard_map(body, mesh=mesh, in_specs=placed, out_specs=P(None, "ra"), check_vma=False)
```

profile of v0, /device:TPU:1, one launch (start us, length us, event | category | flops | bytes accessed | tf_op | source)
XLA Modules:
  0.0 217.3 jit_solution(7903602860294492504)
XLA Ops:
  6.5 0.0 copy-start
  6.5 0.0 all-gather.2.cloned.1.call-start
  6.6 1.4 fusion.2
  8.0 0.4 convert_element_type.52
  8.4 0.0 copy-done
  8.4 2.0 convolution_convert_fusion.1
  10.5 0.0 copy-done.1
  10.5 1.0 convolution_convert_fusion
  11.5 4.1 %pad_maximum_fusion = bf16[16,64,2817]{2,1,0:T(8,128)(2,1)S(1)} fusion(bf16[16,64,1]{2,1,0:T(8,128)(2,1)S(1)} %convert_element_type.52, bf16[16,64,1408]{2,1,0:T(8,128)(2,1)S(1)} %bitcast.7, bf16[16,64,1408]{2,1,0:T(8,128)(2,1)S(1)} %bitcast.6), kind=kLoop, calls=%fused_computation.2 | loop fusion | flops 17307648 | bytes 11538432 | tf_op jit(solution)/shard_map/concatenate | solution.py:22
  15.5 78.1 %all_to_all.16 = bf16[16,64,2817]{2,1,0:T(8,128)(2,1)S(1)} all-to-all(bf16[16,64,2817]{2,1,0:T(8,128)(2,1)S(1)} %pad_maximum_fusion), channel_id=1, replica_groups=mesh['ra'=16,'cb'=8] {'ra'}, dimensions={0} | all-to-all | bytes 11538432 | tf_op jit(solution)/shard_map/all_to_all | solution.py:16
  93.6 0.9 convert_reduce_fusion
  94.5 0.1 fusion.9
  94.6 0.9 fusion.6
  95.5 0.0 all-gather.2.cloned.1.call-update
  95.5 45.0 %all-gather.2.cloned.1.call-done = bf16[1024,1408]{1,0:T(8,128)(2,1)} async-done(((bf16[64,1408]{1,0:T(8,128)(2,1)}), bf16[1024,1408]{1,0:T(8,128)(2,1)}) %all-gather.2.cloned.1.call-update) | async-done | bytes 2883600 | tf_op jit(solution)/shard_map/all_gather | solution.py:64
  140.5 2.8 %convolution_convert_fusion.2 = bf16[1024,256]{1,0:T(8,128)(2,1)S(1)} fusion(bf16[1024,1408]{1,0:T(8,128)(2,1)} %all-gather.2.cloned.1.call-done, bf16[1408,256]{1,0:T(8,128)(2,1)S(1)} %copy-done.5), kind=kOutput, calls=%fused_computation.8 | convolution fusion | flops 738459648 | bytes 4128768 | tf_op jit(solution)/shard_map/dot_general | solution.py:63
  143.3 0.3 broadcast_in_dim.4
  143.6 0.0 copy-start.4
  143.6 54.1 %all_to_all.17 = bf16[8,1024,256]{2,1,0:T(8,128)(2,1)S(1)} all-to-all(bf16[8,1024,256]{2,1,0:T(8,128)(2,1)S(1)} %broadcast_in_dim.4), channel_id=1, replica_groups=mesh['ra'=16,'cb'=8] {'cb'}, dimensions={0} | all-to-all | bytes 8388608 | tf_op jit(solution)/shard_map/all_to_all | solution.py:33
  197.7 0.6 convert_reduce_fusion.1
  198.3 0.2 multiply_reduce_fusion
  198.6 10.7 %all_to_all.18 = f32[16,1,1024]{2,1,0:T(1,128)S(1)} all-to-all(f32[16,1,1024]{2,1,0:T(1,128)S(1)} %broadcast_in_dim.5), channel_id=1, replica_groups=mesh['ra'=16,'cb'=8] {'ra'}, dimensions={0} | all-to-all | bytes 131072 | tf_op jit(solution)/shard_map/all_to_all | solution.py:33
  209.3 0.1 reduce_sum.49
  209.4 1.0 multiply_convert_fusion
  (10 shorter events, 0.1 us)
Async XLA Ops:
  6.5 1.9 copy-start
  6.5 3.9 %copy-start.1 = (bf16[1024,256]{1,0:T(8,128)(2,1)S(1)}, bf16[1024,256]{1,0:T(8,128)(2,1)}, u32[]{:S(2)}) copy-start(bf16[1024,256]{1,0:T(8,128)(2,1)} %param.6) | copy-start | bytes 1572868
  6.5 3.9 %copy-start.3 = (f32[256]{0:T(256)S(1)}, f32[256]{0:T(256)}, u32[]{:S(2)}) copy-start(f32[256]{0:T(256)} %param.7) | copy-start | bytes 3076
  6.5 3.9 %copy-start.2 = (bf16[256,1408]{1,0:T(8,128)(2,1)S(1)}, bf16[256,1408]{1,0:T(8,128)(2,1)}, u32[]{:S(2)}) copy-start(bf16[256,1408]{1,0:T(8,128)(2,1)} %param.9) | copy-start | bytes 2162692
  6.5 134.0 %all-gather.2.cloned.1.call-start = ((), (), s32[]{:S(2)}) async-start(), calls=%async_computation.3 | async-start | bytes 3063808 | tf_op jit(solution)/shard_map/all_gather | solution.py:64
  93.6 46.9 %copy-start.5 = (bf16[1408,256]{1,0:T(8,128)(2,1)S(1)}, bf16[1408,256]{1,0:T(8,128)(2,1)}, u32[]{:S(2)}) copy-start(bf16[1408,256]{1,0:T(8,128)(2,1)} %param.10) | copy-start | bytes 2162692
  143.6 65.8 %copy-start.4 = (f32[256]{0:T(256)S(1)}, f32[256]{0:T(256)}, u32[]{:S(2)}) copy-start(f32[256]{0:T(256)} %param.11) | copy-start | bytes 3076
Sparse Core Ops, SparseCore 0:
  95.6 44.8 all-gather.1
where the time goes:
time: 219 us; the launch traced here: 217 us
  blocking collectives  143 us (65%)
  waiting for transfers between devices  45 us (21%)
  between operations  13.5 us (6%)
  other arithmetic  9.2 us (4%)
  matrix products  5.8 us (3%)
    all_to_all x1, blocking collectives, summed_on_arrival(): pieces = lax.all_to_all(in_blocks(x, dim, length), axis, 0, 0, tiled=True)  78.1 us
    all_to_all x2, blocking collectives, copy_for_each(): lax.all_to_all(jnp.broadcast_to(x[None], (length, *x.shape)), axis, 0, 0,...  64.9 us
    all_gather x1, waiting for transfers between devices, body(): lax.all_gather(hidden, 'ra', axis=0, tiled=True)  45 us
  transfers between devices with their start and end apart: 1, of which 1 were waited for; matrix products, arithmetic and copies ran while one was open for 0% of the time, Pallas kernels for 0%

commit v1 on v0

v1 whole, which is shorter than its diff:
```python
import functools

import jax
import jax.numpy as jnp
from jax import lax
from jax.experimental import pallas as pl
from jax.experimental.pallas import tpu as pltpu
from jax.sharding import PartitionSpec as P

D = 4096
EPS = 1e-06
MESH = pl.DeviceIdType.MESH
F32 = jnp.float32
BF16 = jnp.bfloat16
T = 1024
H = 512
B = 128
W = 256
L = 128
K = 3

RA = [(dz, dy) for dz in range(4) for dy in range(4) if (dz, dy) != (0, 0)]
PLANE = [(dx, dy) for dx in range(4) for dy in range(4) if (dx, dy) != (0, 0)]


def far_first(pairs):
    return sorted(pairs, key=lambda p: -(min(p[0], 4 - p[0]) + min(p[1], 4 - p[1])))


def mod4(v):
    return lax.rem(v + 4, 4)


def row_sums(v):
    sq = v * v
    hi = sq.astype(BF16)
    lo = (sq - hi.astype(F32)).astype(BF16)
    ones = jnp.ones((8, v.shape[1]), BF16)
    dims = (((1,), (1,)), ((), ()))
    out = lax.dot_general(ones, hi, dims, preferred_element_type=F32)
    return out + lax.dot_general(ones, lo, dims, preferred_element_type=F32)


def as_columns(row):
    return jnp.transpose(jnp.broadcast_to(row[:1], (L, L)), (1, 0))


def kernel(
    tok, gain, wg, wu, wd, ogain, out,
    xg, wb, wdb, part, rbuf, hall, psend, precv, sq_s, sq_r, st_s, st_r,
    loc, x_ss, x_rs, w_ss, w_rs, f_ss, f_rs, d_ss, d_rs, df_ss, df_rs,
    r_ss, r_rs, h_ss, h_rs, p_ss, p_rs, q_ss, q_rs, t_ss, t_rs, o_ss, o_rs, of_ss, of_rs,
):
    ra, cb = lax.axis_index("ra"), lax.axis_index("cb")
    z, y, x, c = ra // 4, lax.rem(ra, 4), cb // 2, lax.rem(cb, 2)

    def dev(dz=0, dy=0, dx=0, dc=0):
        return (mod4(z + dz) * 4 + mod4(y + dy), mod4(x + dx) * 2 + lax.rem(c + dc, 2))

    sends = []

    def send(src, dst, ss, rs, to):
        cp = pltpu.make_async_remote_copy(
            src_ref=src, dst_ref=dst, send_sem=ss, recv_sem=rs, device_id=to, device_id_type=MESH
        )
        cp.start()
        sends.append(cp)
        return cp

    def local(src, dst, sem):
        cp = pltpu.make_async_copy(src, dst, sem)
        cp.start()
        return cp

    partners = [dev(dz, dy) for dz, dy in RA] + [dev(0, dy, dx) for dx, dy in PLANE if dx] + [dev(dc=1)]
    bar = pltpu.get_barrier_semaphore()
    for p in partners:
        pl.semaphore_signal(bar, inc=1, device_id=p, device_id_type=MESH)

    def tile0(yy):
        return jnp.minimum(3 * yy, 8)

    def cols(yy, k):
        return pl.ds(pl.multiple_of((tile0(yy) + k) * L, L), L)

    mine = pl.ds(pl.multiple_of(c * H, H), H)
    locals_w = []
    for k in range(K):
        locals_w.append(local(wg.at[:, cols(y, k)], wb.at[k, c, 0, :, :L], loc.at[2 * k]))
        locals_w.append(local(wu.at[:, cols(y, k)], wb.at[k, c, 0, :, L:], loc.at[2 * k + 1]))
    local_d = local(wd.at[pl.ds(tile0(y), K)], wdb.at[y, :, c], loc.at[2 * K])

    t32 = tok[mine, :].astype(F32)
    xg[0] = (t32 * gain[...]).astype(BF16)
    sq = row_sums(t32)
    for b in range(4):
        sq_s[b] = sq[:, b * L : (b + 1) * L]

    pl.semaphore_wait(bar, len(partners))

    near = (2, 1, 3)
    xs = {d: send(xg.at[0], xg.at[d], x_ss.at[d], x_rs.at[d], dev(dy=d)) for d in near}
    ws = {}
    for k in range(K):
        for d in near:
            yy = mod4(y + d)
            ws[k, d, 0] = send(wg.at[:, cols(yy, k)], wb.at[k, c, d, :, :L], w_ss.at[k, d, 0], w_rs.at[k, d, 0], dev(dy=d))
            ws[k, d, 1] = send(wu.at[:, cols(yy, k)], wb.at[k, c, d, :, L:], w_ss.at[k, d, 1], w_rs.at[k, d, 1], dev(dy=d))
        if k == 0:
            qs = [
                send(sq_s.at[mod4(z + dz)], sq_r.at[i], q_ss.at[i], q_rs.at[i], dev(dz, dy))
                for i, (dz, dy) in enumerate(RA)
            ]
    ds_ = {
        d: send(wd.at[pl.ds(tile0(mod4(y + d)), K)], wdb.at[y, :, c], d_ss.at[d], d_rs.at[d], dev(dy=d))
        for d in near
    }

    inv = None
    hs = {}
    rs = {}

    def hidden_of(k):
        for d in near:
            rs[k, d].wait_recv()
        own = part[k, pl.ds(pl.multiple_of(z * B, B), B), :].astype(F32)
        total = own
        for d in range(3):
            total = total + rbuf[k, d].astype(F32)
        for cc in range(2):
            gate = total[:, 2 * cc * L : (2 * cc + 1) * L] * inv
            up = total[:, (2 * cc + 1) * L : (2 * cc + 2) * L] * inv
            hid = gate / (1.0 + jnp.exp(-gate)) * up
            if k == 0:
                hid = jnp.where(y == 3, jnp.zeros_like(hid), hid)
            hall[pl.ds(pl.multiple_of(z * B, B), B), (2 * k + cc) * L : (2 * k + cc + 1) * L] = hid.astype(BF16)
        block = hall.at[pl.ds(pl.multiple_of(z * B, B), B), 2 * k * L : (2 * k + 2) * L]
        for d in near:
            hs[k, d] = send(block, block, h_ss.at[k, d], h_rs.at[k, d], dev(dz=d))

    for d in near:
        xs[d].wait_recv()
    for k in range(K):
        fs = []
        for d in (0,) + near:
            if d == 0:
                locals_w[2 * k].wait()
                locals_w[2 * k + 1].wait()
            else:
                ws[k, d, 0].wait_recv()
                ws[k, d, 1].wait_recv()
            fs.append(send(wb.at[k, c, d], wb.at[k, c, d], f_ss.at[k, d], f_rs.at[k, d], dev(dc=1)))
        for turn in range(2):
            cc = lax.rem(c + turn, 2)
            if turn == 1:
                for f in fs:
                    f.wait_recv()
            acc = jnp.zeros((H, 2 * L), F32)
            for d in range(4):
                acc = acc + jnp.dot(xg[d], wb[k, cc, d], preferred_element_type=F32)
            lanes = pl.ds(pl.multiple_of(cc * 2 * L, 2 * L), 2 * L)
            part[k, :, lanes] = acc.astype(BF16)
        for d in near:
            zz = pl.ds(pl.multiple_of(mod4(z + d) * B, B), B)
            rs[k, d] = send(part.at[k, zz, :], rbuf.at[k, d - 1], r_ss.at[k, d], r_rs.at[k, d], dev(dz=d))
        if k == 0:
            total = sq_s[z]
            for i, q in enumerate(qs):
                q.wait_recv()
                total = total + sq_r[i]
            inv = as_columns(lax.rsqrt(total / D + EPS))
        else:
            hidden_of(k - 1)

    dfs = []
    for d in (0,) + near:
        if d == 0:
            local_d.wait()
        else:
            ds_[d].wait_recv()
        block = wdb.at[mod4(y - d), :, c]
        dfs.append(send(block, block, df_ss.at[d], df_rs.at[d], dev(dc=1)))
    hidden_of(K - 1)
    for f in dfs:
        f.wait_recv()
    for k in range(K):
        for d in near:
            hs[k, d].wait_recv()

    ps = {}
    for dy in (2, 1, 3, 0):
        yy = mod4(y + dy)
        acc = jnp.dot(hall[...], wdb[yy].reshape(2 * K * L, W), preferred_element_type=F32)
        psend[yy] = acc.astype(BF16)
        for i, (dx, dyy) in enumerate(PLANE):
            if dyy == dy:
                xx = pl.ds(pl.multiple_of(mod4(x + dx) * B, B), B)
                ps[i] = send(psend.at[yy, xx, :], precv.at[i], p_ss.at[i], p_rs.at[i], dev(dy=dy, dx=dx))
    piece = pl.ds(pl.multiple_of(c * H + x * B, B), B)
    stream = 0.5 * tok[piece, :].astype(F32) + psend[y, pl.ds(pl.multiple_of(x * B, B), B), :].astype(F32)
    for i in range(len(PLANE)):
        ps[i].wait_recv()
        stream = stream + precv[i].astype(F32)
    st_s[...] = row_sums(stream)
    ts = [
        send(st_s, st_r.at[i], t_ss.at[i], t_rs.at[i], dev(dz, dy)) for i, (dz, dy) in enumerate(RA)
    ]
    total = st_s[...]
    for i, t in enumerate(ts):
        t.wait_recv()
        total = total + st_r[i]
    factor = as_columns(lax.rsqrt(total / D + EPS))
    for h in range(2):
        lanes = slice(h * L, (h + 1) * L)
        out[piece, lanes] = (stream[:, lanes] * factor * ogain[:, lanes]).astype(BF16)

    os_ = {d: send(out.at[piece, :], out.at[piece, :], o_ss.at[d], o_rs.at[d], dev(dx=d)) for d in near}
    ofs = []
    for d in (0,) + near:
        if d:
            os_[d].wait_recv()
        rows = pl.ds(pl.multiple_of(c * H + mod4(x - d) * B, B), B)
        ofs.append(send(out.at[rows, :], out.at[rows, :], of_ss.at[d], of_rs.at[d], dev(dc=1)))
    for f in ofs:
        f.wait_recv()
    for s in sends:
        s.wait_send()


def body(tokens, norm_gain, gate_weight, up_weight, down_weight, out_gain):
    dma = pltpu.SemaphoreType.DMA
    vmem = pl.BlockSpec(memory_space=pltpu.VMEM)
    hbm = pl.BlockSpec(memory_space=pl.ANY)
    n = len(RA)
    return pl.pallas_call(
        kernel,
        out_shape=jax.ShapeDtypeStruct((T, W), BF16),
        in_specs=[vmem, vmem, hbm, hbm, hbm, vmem],
        out_specs=vmem,
        scratch_shapes=[
            pltpu.VMEM((4, H, W), BF16),
            pltpu.VMEM((K, 2, 4, W, 2 * L), BF16),
            pltpu.VMEM((4, K, 2, L, W), BF16),
            pltpu.VMEM((K, H, 4 * L), BF16),
            pltpu.VMEM((K, 3, B, 4 * L), BF16),
            pltpu.VMEM((H, 2 * K * L), BF16),
            pltpu.VMEM((4, H, W), BF16),
            pltpu.VMEM((n, B, W), BF16),
            pltpu.VMEM((4, 8, L), F32),
            pltpu.VMEM((n, 8, L), F32),
            pltpu.VMEM((8, L), F32),
            pltpu.VMEM((n, 8, L), F32),
            dma((2 * K + 1,)),
            dma((4,)), dma((4,)),
            dma((K, 4, 2)), dma((K, 4, 2)),
            dma((K, 4)), dma((K, 4)),
            dma((4,)), dma((4,)),
            dma((4,)), dma((4,)),
            dma((K, 4)), dma((K, 4)),
            dma((K, 4)), dma((K, 4)),
            dma((n,)), dma((n,)),
            dma((n,)), dma((n,)),
            dma((n,)), dma((n,)),
            dma((4,)), dma((4,)),
            dma((4,)), dma((4,)),
        ],
        compiler_params=pltpu.CompilerParams(
            collective_id=0, has_side_effects=True, vmem_limit_bytes=40 * 1024 * 1024
        ),
    )(
        tokens,
        norm_gain.reshape(1, W),
        gate_weight,
        up_weight,
        down_weight.reshape(11, L, W),
        out_gain.reshape(1, W),
    )


def solution(mesh):
    placed = (P(None, "ra"), P("ra"), P("ra", "cb"), P("ra", "cb"), P("cb", "ra"), P("ra"))
    return jax.shard_map(body, mesh=mesh, in_specs=placed, out_specs=P(None, "ra"), check_vma=False)
```

time: 219 us -> 95.2 us (0.43)
  blocking collectives: 143 us -> 0 us
  Pallas kernels: 0 us -> 89.1 us
  waiting for transfers between devices: 45 us -> 0 us
  between operations: 13.5 us -> 0.02 us
  other arithmetic: 9.2 us -> 0 us
  matrix products: 5.8 us -> 0 us
  local copies, waits for them, and re-layouts: 0.77 us -> 5.86 us
    all_to_all x3 -> x0, blocking collectives: 143 us -> none  [the longest x1 78.1 us: summed_on_arrival(): pieces = lax.all_to_all(in_blocks(x, dim, length), axis, 0, 0, tiled=True)]
    pallas_call x0 -> x1, Pallas kernels: none -> 89.1 us  [body(): pl.pallas_call(kernel, out_shape=jax.ShapeDtypeStruct((T, W), BF16), in_s...]
    all_gather x1 -> x0, waiting for transfers between devices: 45 us -> none  [body(): lax.all_gather(hidden, 'ra', axis=0, tiled=True)]
    unnamed x12 -> x13, local copies, waits for them, and re-layouts: 0.03 us -> 5.86 us
    dot_general x3 -> x0, matrix products: 5.8 us -> none  [the longest x1 2.79 us: body(): jnp.dot(lax.all_gather(hidden, 'ra', axis=0, tiled=True), down_weight, pr...]
    concatenate x1 -> x0, other arithmetic: 4.06 us -> none  [sent_together(): both = jnp.concatenate(columns, axis=along)]
    reduce_sum x5 -> x0, other arithmetic: 3.13 us -> none  [the longest x1 1.39 us: body(): local_sq = jnp.sum(stream_in * stream_in, axis=1)]
  transfers between devices with their start and end apart: 1 -> 0, of which waited for: 1 -> 0; matrix products, arithmetic and copies ran while one was open for 0% -> 0% of each run, Pallas kernels for 0% -> 0%
where the time goes in v1:
time: 95.2 us; the launch traced here: 94.9 us
  Pallas kernels  89.1 us (94%)
  local copies, waits for them, and re-layouts  5.86 us (6%)
    pallas_call x1, Pallas kernels, body(): pl.pallas_call(kernel, out_shape=jax.ShapeDtypeStruct((T, W), BF16), in_s...  89.1 us
    unnamed x13, local copies, waits for them, and re-layouts  5.86 us

profile of v1, /device:TPU:1, one launch (start us, length us, event | category | flops | bytes accessed | tf_op | source)
XLA Modules:
  0.0 94.9 jit_solution(1450934463461719075)
XLA Ops:
  0.0 0.0 copy-start.5
  0.0 0.0 copy-start.4
  0.0 0.7 copy-done.5
  0.7 0.0 copy-done.4
  0.7 0.0 copy-start
  0.7 1.1 %copy-done = bf16[256,1408]{1,0:T(8,128)(2,1)S(1)} copy-done((bf16[256,1408]{1,0:T(8,128)(2,1)S(1)}, bf16[256,1408]{1,0:T(8,128)(2,1)}, u32[]{:S(2)}) %copy-start) | copy-done | bytes 720920
  1.8 0.0 copy-start.1
  1.8 1.1 %copy-done.1 = bf16[256,1408]{1,0:T(8,128)(2,1)S(1)} copy-done((bf16[256,1408]{1,0:T(8,128)(2,1)S(1)}, bf16[256,1408]{1,0:T(8,128)(2,1)}, u32[]{:S(2)}) %copy-start.1) | copy-done | bytes 720920
  2.9 0.0 copy-start.2
  2.9 1.1 %copy-done.2 = bf16[1408,256]{1,0:T(8,128)(2,1)S(1)} copy-done((bf16[1408,256]{1,0:T(8,128)(2,1)S(1)}, bf16[1408,256]{1,0:T(8,128)(2,1)}, u32[]{:S(2)}) %copy-start.2) | copy-done | bytes 720920
  4.0 0.0 copy-start.3
  4.0 1.0 %copy-done.3 = bf16[1024,256]{1,0:T(8,128)(2,1)S(1)} copy-done((bf16[1024,256]{1,0:T(8,128)(2,1)S(1)}, bf16[1024,256]{1,0:T(8,128)(2,1)}, u32[]{:S(2)}) %copy-start.3) | copy-done | bytes 524312
  5.1 89.1 %shard_map.64 = bf16[1024,256]{1,0:T(8,128)(2,1)S(1)} custom-call(bf16[1024,256]{1,0:T(8,128)(2,1)S(1)} %copy-done.3, f32[1,256]{1,0:T(1,128)S(1)} %bitcast.4, bf16[256,1408]{1,0:T(8,128)(2,1)S(1)} %copy-done, bf16[256,1408]{1,0:T(8,128)(2,1)S(1)} %copy-done.1, bf16[11,128,256]{2,1,0:T(8,128)(2,1)S(1)} %bitcast.3, f32[1,256]{1,0:T(1,128)S(1)} %bitcast.5), custom_call_target="tpu_custom_call" | custom-call | tf_op jit(solution)/shard_map/pallas_call | solution.py:235
  94.1 0.8 copy.8
Async XLA Ops:
  0.0 0.7 copy-start.5
  0.0 0.7 copy-start.4
  0.7 1.1 %copy-start = (bf16[256,1408]{1,0:T(8,128)(2,1)S(1)}, bf16[256,1408]{1,0:T(8,128)(2,1)}, u32[]{:S(2)}) copy-start(bf16[256,1408]{1,0:T(8,128)(2,1)} %wg.1) | copy-start | bytes 2162692
  1.8 1.1 %copy-start.1 = (bf16[256,1408]{1,0:T(8,128)(2,1)S(1)}, bf16[256,1408]{1,0:T(8,128)(2,1)}, u32[]{:S(2)}) copy-start(bf16[256,1408]{1,0:T(8,128)(2,1)} %wu.1) | copy-start | bytes 2162692
  2.9 1.1 %copy-start.2 = (bf16[1408,256]{1,0:T(8,128)(2,1)S(1)}, bf16[1408,256]{1,0:T(8,128)(2,1)}, u32[]{:S(2)}) copy-start(bf16[1408,256]{1,0:T(8,128)(2,1)} %param.10) | copy-start | bytes 2162692
  4.0 1.0 %copy-start.3 = (bf16[1024,256]{1,0:T(8,128)(2,1)S(1)}, bf16[1024,256]{1,0:T(8,128)(2,1)}, u32[]{:S(2)}) copy-start(bf16[1024,256]{1,0:T(8,128)(2,1)} %tok.1) | copy-start | bytes 1572868

commit v2 on v1

v2 whole, which is shorter than its diff:
```python
import functools

import jax
import jax.numpy as jnp
from jax import lax
from jax.experimental import pallas as pl
from jax.experimental.pallas import tpu as pltpu
from jax.sharding import PartitionSpec as P

D = 4096
EPS = 1e-06
MESH = pl.DeviceIdType.MESH
scope = jax.named_scope
F32 = jnp.float32
BF16 = jnp.bfloat16
T = 1024
H = 512
B = 128
W = 256
L = 128
K = 3

R = 96

NEAR = (2, 1, 3)
ROW = [(d, e) for d in (2, 1, 3) for e in range(2)] + [(0, 1)]


def mod4(v):
    return lax.rem(v + 4, 4)


def row_sums(v):
    sq = v * v
    hi = sq.astype(BF16)
    lo = (sq - hi.astype(F32)).astype(BF16)
    ones = jnp.ones((8, v.shape[1]), BF16)
    dims = (((1,), (1,)), ((), ()))
    out = lax.dot_general(ones, hi, dims, preferred_element_type=F32)
    return out + lax.dot_general(ones, lo, dims, preferred_element_type=F32)


def as_columns(row):
    return jnp.transpose(jnp.broadcast_to(row[:1], (L, L)), (1, 0))


def kernel(
    tok_h, gain_h, wg_h, wu_h, wd_h, ogain_h, out,
    tok, gain, wg, wu, wd, ogain, xg, wb, wdb, part, rbuf, hall, psend, p1, p2, s1, s2, p3, p4,
    sq_s, sq_r, sq2_r, st_s, st_r, st2_s, st2_r, st3_r,
    head, loc, xa_ss, xa_rs, xb_ss, xb_rs, xc_ss, xc_rs, w_ss, w_rs, f_ss, f_rs, d_ss, d_rs, df_ss, df_rs,
    r_ss, r_rs, h_ss, h_rs, p1_ss, p1_rs, p2_ss, p2_rs, p3_ss, p3_rs, p4_ss, p4_rs,
    q_ss, q_rs, q2_ss, q2_rs, t_ss, t_rs, t2_ss, t2_rs, t3_ss, t3_rs, o_ss, o_rs, of_ss, of_rs,
):
    ra, cb = lax.axis_index("ra"), lax.axis_index("cb")
    z, y, x, c = ra // 4, lax.rem(ra, 4), cb // 2, lax.rem(cb, 2)

    def dev(dz=0, dy=0, dx=0, dc=0):
        return (mod4(z + dz) * 4 + mod4(y + dy), mod4(x + dx) * 2 + lax.rem(c + dc, 2))

    sends = []

    def send(src, dst, ss, rs, to):
        cp = pltpu.make_async_remote_copy(
            src_ref=src, dst_ref=dst, send_sem=ss, recv_sem=rs, device_id=to, device_id_type=MESH
        )
        cp.start()
        sends.append(cp)
        return cp

    def local(src, dst, sem):
        cp = pltpu.make_async_copy(src, dst, sem)
        cp.start()
        return cp

    partners = [dev(dy=d) for d in NEAR] + [dev(dz=d) for d in NEAR] + [dev(dx=d, dc=e) for d, e in ROW]
    bar = pltpu.get_barrier_semaphore()
    for p in partners:
        pl.semaphore_signal(bar, inc=1, device_id=p, device_id_type=MESH)

    heads = [
        local(src, dst, head.at[i])
        for i, (src, dst) in enumerate(
            ((tok_h, tok), (gain_h, gain), (wg_h, wg), (wu_h, wu), (wd_h, wd), (ogain_h, ogain))
        )
    ]

    def tile0(yy):
        return jnp.minimum(3 * yy, 8)

    def cols(yy, k):
        return pl.ds(pl.multiple_of((tile0(yy) + k) * L, L), L)

    def rows(start, size):
        return pl.ds(pl.multiple_of(start, 16), size)

    locals_w = []
    for k in range(K):
        locals_w.append(local(wg_h.at[:, cols(y, k)], wb.at[k, c, 0, :, :L], loc.at[2 * k]))
        locals_w.append(local(wu_h.at[:, cols(y, k)], wb.at[k, c, 0, :, L:], loc.at[2 * k + 1]))
    local_d = local(wd_h.at[pl.ds(tile0(y), K)], wdb.at[y, :, c], loc.at[2 * K])

    heads[0].wait()
    heads[1].wait()
    t32 = tok[rows(c * H, H), :].astype(F32)
    xg[0] = (t32 * gain[...]).astype(BF16)
    sq = row_sums(t32)
    for b in range(4):
        sq_s[b] = sq[:, b * L : (b + 1) * L]
    for h in heads[2:]:
        h.wait()
    with scope("barrier"):
        pl.semaphore_wait(bar, len(partners))

    quarter = rows(x * R, R)
    rest = slice(4 * R, H)
    xa = {d: send(xg.at[0, quarter], xg.at[d, quarter], xa_ss.at[d], xa_rs.at[d], dev(dy=d)) for d in NEAR}
    xb = {d: send(xg.at[0, rest], xg.at[d, rest], xb_ss.at[d], xb_rs.at[d], dev(dy=d)) for d in NEAR}
    qs = {d: send(sq_s, sq_r.at[d - 1], q_ss.at[d], q_rs.at[d], dev(dy=d)) for d in NEAR}
    ws = {}
    for k in range(K):
        for d in NEAR:
            yy = mod4(y + d)
            ws[k, d, 0] = send(wg.at[:, cols(yy, k)], wb.at[k, c, d, :, :L], w_ss.at[k, d, 0], w_rs.at[k, d, 0], dev(dy=d))
            ws[k, d, 1] = send(wu.at[:, cols(yy, k)], wb.at[k, c, d, :, L:], w_ss.at[k, d, 1], w_rs.at[k, d, 1], dev(dy=d))
    ds_ = {
        d: send(wd.at[pl.ds(tile0(mod4(y + d)), K)], wdb.at[y, :, c], d_ss.at[d], d_rs.at[d], dev(dy=d))
        for d in NEAR
    }
    xc = {}
    for d in (1, 3, 2):
        with scope(f"wait_xa#d={d}"):
            xa[d].wait_recv()
        for e in NEAR:
            xc[d, e] = send(xg.at[d, quarter], xg.at[d, quarter], xc_ss.at[d, e], xc_rs.at[d, e], dev(dx=e))
    with scope("wait_xb"):
        for d in NEAR:
            xb[d].wait_recv()
    with scope("wait_sq"):
        for d in NEAR:
            qs[d].wait_recv()
    for b in range(4):
        sq_s2 = sq_s[b] + sq_r[0, b] + sq_r[1, b] + sq_r[2, b]
        st2_s[b] = sq_s2
    q2 = {d: send(st2_s.at[mod4(z + d)], sq2_r.at[d - 1], q2_ss.at[d], q2_rs.at[d], dev(dz=d)) for d in NEAR}

    inv = None
    hs = {}
    rs = {}
    fs = {}
    own_rows = rows(z * B, B)

    def columns_of(k):
        with scope(f"wait_w#k={k}"):
            for d in (0,) + NEAR:
                if d == 0:
                    locals_w[2 * k].wait()
                    locals_w[2 * k + 1].wait()
                else:
                    ws[k, d, 0].wait_recv()
                    ws[k, d, 1].wait_recv()
                fs[k, d] = send(wb.at[k, c, d], wb.at[k, c, d], f_ss.at[k, d], f_rs.at[k, d], dev(dc=1))

    def hidden_of(k):
        with scope(f"wait_rs#k={k}"):
            for d in NEAR:
                rs[k, d].wait_recv()
        total = part[k, own_rows, :].astype(F32)
        for d in range(3):
            total = total + rbuf[k, d].astype(F32)
        for cc in range(2):
            gate = total[:, 2 * cc * L : (2 * cc + 1) * L] * inv
            up = total[:, (2 * cc + 1) * L : (2 * cc + 2) * L] * inv
            hid = gate / (1.0 + jnp.exp(-gate)) * up
            if k == 0:
                hid = jnp.where(y == 3, jnp.zeros_like(hid), hid)
            hall[own_rows, (2 * k + cc) * L : (2 * k + cc + 1) * L] = hid.astype(BF16)
        block = hall.at[own_rows, 2 * k * L : (2 * k + 2) * L]
        for d in NEAR:
            hs[k, d] = send(block, block, h_ss.at[k, d], h_rs.at[k, d], dev(dz=d))

    columns_of(0)
    with scope("wait_xc"):
        for d in NEAR:
            for e in NEAR:
                xc[d, e].wait_recv()
    for k in range(K):
        if k:
            columns_of(k)
        for turn in range(2):
            cc = lax.rem(c + turn, 2)
            if turn == 1:
                with scope(f"wait_f#k={k}"):
                    for d in (0,) + NEAR:
                        fs[k, d].wait_recv()
            acc = jnp.zeros((H, 2 * L), F32)
            for d in range(4):
                acc = acc + jnp.dot(xg[d], wb[k, cc, d], preferred_element_type=F32)
            lanes = pl.ds(pl.multiple_of(cc * 2 * L, 2 * L), 2 * L)
            part[k, :, lanes] = acc.astype(BF16)
        for d in NEAR:
            zz = rows(mod4(z + d) * B, B)
            rs[k, d] = send(part.at[k, zz, :], rbuf.at[k, d - 1], r_ss.at[k, d], r_rs.at[k, d], dev(dz=d))
        if k == 0:
            with scope("wait_sq2"):
                for d in NEAR:
                    q2[d].wait_recv()
            total = st2_s[z] + sq2_r[0] + sq2_r[1] + sq2_r[2]
            inv = as_columns(lax.rsqrt(total / D + EPS))
        else:
            hidden_of(k - 1)

    dfs = []
    with scope("wait_d"):
        for d in (0,) + NEAR:
            if d == 0:
                local_d.wait()
            else:
                ds_[d].wait_recv()
            block = wdb.at[mod4(y - d), :, c]
            dfs.append(send(block, block, df_ss.at[d], df_rs.at[d], dev(dc=1)))
    hidden_of(K - 1)
    with scope("wait_df"):
        for f in dfs:
            f.wait_recv()
    with scope("wait_h"):
        for k in range(K):
            for d in NEAR:
                hs[k, d].wait_recv()

    a1, a2, a3, a4 = {}, {}, {}, {}
    for dy in (2, 1, 3, 0):
        yy = mod4(y + dy)
        acc = jnp.dot(hall[...], wdb[yy].reshape(2 * K * L, W), preferred_element_type=F32)
        psend[yy] = acc.astype(BF16).reshape(4, 2, B // 2, W)
        if dy:
            a1[dy] = send(psend.at[yy, :, 0], p1.at[dy - 1], p1_ss.at[dy], p1_rs.at[dy], dev(dy=dy))
        for dx in NEAR:
            a2[dx, dy] = send(psend.at[yy, mod4(x + dx), 1], p2.at[dx - 1, yy], p2_ss.at[dx, dy], p2_rs.at[dx, dy], dev(dx=dx))
    with scope("wait_p1"):
        for d in NEAR:
            a1[d].wait_recv()
    for xx in range(4):
        v = psend[y, xx, 0].astype(F32)
        for d in range(3):
            v = v + p1[d, xx].astype(F32)
        s1[xx] = v.astype(BF16)
    for d in NEAR:
        a3[d] = send(s1.at[mod4(x + d)], p3.at[d - 1], p3_ss.at[d], p3_rs.at[d], dev(dx=d))
    with scope("wait_p2"):
        for dx in NEAR:
            for dy in range(4):
                a2[dx, dy].wait_recv()
    for yy in range(4):
        v = psend[yy, x, 1].astype(F32)
        for d in range(3):
            v = v + p2[d, yy].astype(F32)
        s2[yy] = v.astype(BF16)
    for d in NEAR:
        a4[d] = send(s2.at[mod4(y + d)], p4.at[d - 1], p4_ss.at[d], p4_rs.at[d], dev(dy=d))
    piece = c * H + x * B
    with scope("wait_p3"):
        for d in NEAR:
            a3[d].wait_recv()
    v1 = s1[x].astype(F32)
    for d in range(3):
        v1 = v1 + p3[d].astype(F32)
    with scope("wait_p4"):
        for d in NEAR:
            a4[d].wait_recv()
    v2 = s2[y].astype(F32)
    for d in range(3):
        v2 = v2 + p4[d].astype(F32)
    stream = 0.5 * tok[rows(piece, B), :].astype(F32) + jnp.concatenate([v1, v2], axis=0)
    out[rows(piece, B), :] = stream.astype(BF16)

    ag = {d: send(out.at[rows(piece, B), :], out.at[rows(piece, B), :], o_ss.at[d], o_rs.at[d], dev(dx=d)) for d in NEAR}
    st_s[...] = row_sums(stream)
    ts = {d: send(st_s, st_r.at[d - 1], t_ss.at[d], t_rs.at[d], dev(dz=d)) for d in NEAR}
    with scope("wait_st"):
        for d in NEAR:
            ts[d].wait_recv()
    st3_r[8] = st_s[...] + st_r[0] + st_r[1] + st_r[2]
    t2 = {d: send(st3_r.at[8], st2_r.at[d - 1], t2_ss.at[d], t2_rs.at[d], dev(dy=d)) for d in NEAR}
    with scope("wait_st2"):
        for d in NEAR:
            t2[d].wait_recv()
    st3_r[2 * x + c] = st3_r[8] + st2_r[0] + st2_r[1] + st2_r[2]
    me = st3_r.at[2 * x + c]
    t3 = [send(me, me, t3_ss.at[i], t3_rs.at[i], dev(dx=d, dc=e)) for i, (d, e) in enumerate(ROW)]
    ofs = []
    with scope("wait_o"):
        for d in (0,) + NEAR:
            if d:
                ag[d].wait_recv()
            block = out.at[rows(c * H + mod4(x - d) * B, B), :]
            ofs.append(send(block, block, of_ss.at[d], of_rs.at[d], dev(dc=1)))
    with scope("wait_of"):
        for f in ofs:
            f.wait_recv()
    with scope("wait_st3"):
        for t in t3:
            t.wait_recv()
    with scope("wait_sends"):
        for s in sends:
            s.wait_send()
    for xx in range(4):
        for cc in range(2):
            factor = as_columns(lax.rsqrt(st3_r[2 * xx + cc] / D + EPS))
            r = slice(cc * H + xx * B, cc * H + (xx + 1) * B)
            for h in range(2):
                lanes = slice(h * L, (h + 1) * L)
                out[r, lanes] = (out[r, lanes].astype(F32) * factor * ogain[:, lanes]).astype(BF16)


def body(tokens, norm_gain, gate_weight, up_weight, down_weight, out_gain):
    dma = pltpu.SemaphoreType.DMA
    hbm = pl.BlockSpec(memory_space=pltpu.HBM)
    operands = (
        tokens,
        norm_gain.reshape(1, W),
        gate_weight,
        up_weight,
        down_weight.reshape(11, L, W),
        out_gain.reshape(1, W),
    )
    pair = lambda *shape: (dma(shape), dma(shape))
    return pl.pallas_call(
        kernel,
        out_shape=jax.ShapeDtypeStruct((T, W), BF16),
        in_specs=[hbm] * 6,
        out_specs=pl.BlockSpec(memory_space=pltpu.VMEM),
        scratch_shapes=[
            pltpu.VMEM((T, W), BF16),
            pltpu.VMEM((1, W), F32),
            pltpu.VMEM((W, 11 * L), BF16),
            pltpu.VMEM((W, 11 * L), BF16),
            pltpu.VMEM((11, L, W), BF16),
            pltpu.VMEM((1, W), F32),
            pltpu.VMEM((4, H, W), BF16),
            pltpu.VMEM((K, 2, 4, W, 2 * L), BF16),
            pltpu.VMEM((4, K, 2, L, W), BF16),
            pltpu.VMEM((K, H, 4 * L), BF16),
            pltpu.VMEM((K, 3, B, 4 * L), BF16),
            pltpu.VMEM((H, 2 * K * L), BF16),
            pltpu.VMEM((4, 4, 2, B // 2, W), BF16),
            pltpu.VMEM((3, 4, B // 2, W), BF16),
            pltpu.VMEM((3, 4, B // 2, W), BF16),
            pltpu.VMEM((4, B // 2, W), BF16),
            pltpu.VMEM((4, B // 2, W), BF16),
            pltpu.VMEM((3, B // 2, W), BF16),
            pltpu.VMEM((3, B // 2, W), BF16),
            pltpu.VMEM((4, 8, L), F32),
            pltpu.VMEM((3, 4, 8, L), F32),
            pltpu.VMEM((3, 8, L), F32),
            pltpu.VMEM((8, L), F32),
            pltpu.VMEM((3, 8, L), F32),
            pltpu.VMEM((4, 8, L), F32),
            pltpu.VMEM((3, 8, L), F32),
            pltpu.VMEM((9, 8, L), F32),
            dma((6,)),
            dma((2 * K + 1,)),
            *pair(4), *pair(4), *pair(4, 4),
            *pair(K, 4, 2), *pair(K, 4), *pair(4), *pair(4),
            *pair(K, 4), *pair(K, 4),
            *pair(4), *pair(4, 4), *pair(4), *pair(4),
            *pair(4), *pair(4),
            *pair(4), *pair(4), *pair(7),
            *pair(4), *pair(4),
        ],
        compiler_params=pltpu.CompilerParams(
            collective_id=0, has_side_effects=True, vmem_limit_bytes=40 * 1024 * 1024
        ),
    )(*[pltpu.with_memory_space_constraint(a, pltpu.HBM) for a in operands])


def solution(mesh):
    placed = (P(None, "ra"), P("ra"), P("ra", "cb"), P("ra", "cb"), P("cb", "ra"), P("ra"))
    return jax.shard_map(body, mesh=mesh, in_specs=placed, out_specs=P(None, "ra"), check_vma=False)
```

time: 95.2 us -> 80.2 us (0.84)
  Pallas kernels: 89.1 us -> 79.3 us
  local copies, waits for them, and re-layouts: 5.86 us -> 0.8 us
    pallas_call x1, Pallas kernels: 89.1 us -> 79.3 us  [body(): pl.pallas_call(kernel, out_shape=jax.ShapeDtypeStruct((T, W), BF16), in_s...]
    unnamed x13 -> x1, local copies, waits for them, and re-layouts: 5.86 us -> 0.8 us
where the time goes in v2:
time: 80.2 us; the launch traced here: 80.1 us
  Pallas kernels  79.3 us (99%)
    pallas_call x1, Pallas kernels, body(): pl.pallas_call(kernel, out_shape=jax.ShapeDtypeStruct((T, W), BF16), in_s...  79.3 us

profile of v2, /device:TPU:1, one launch (start us, length us, event | category | flops | bytes accessed | tf_op | source)
XLA Modules:
  0.0 80.1 jit_solution(794709482800343796)
XLA Ops:
  0.0 79.3 %shard_map.64 = bf16[1024,256]{1,0:T(8,128)(2,1)S(1)} custom-call(bf16[1024,256]{1,0:T(8,128)(2,1)} %tok_h.1, f32[1,256]{1,0:T(1,128)} %bitcast.4, bf16[256,1408]{1,0:T(8,128)(2,1)} %wg_h.1, bf16[256,1408]{1,0:T(8,128)(2,1)} %wu_h.1, bf16[11,128,256]{2,1,0:T(8,128)(2,1)} %bitcast.3, f32[1,256]{1,0:T(1,128)} %bitcast.5), custom_call_target="tpu_custom_call" | custom-call | tf_op jit(solution)/shard_map/pallas_call | solution.py:328
  79.3 0.8 copy.8

commit v3 on v2

v3 whole, which is shorter than its diff:
```python
import functools

import jax
import jax.numpy as jnp
from jax import lax
from jax.experimental import pallas as pl
from jax.experimental.pallas import tpu as pltpu
from jax.sharding import PartitionSpec as P

D = 4096
EPS = 1e-06
MESH = pl.DeviceIdType.MESH
scope = jax.named_scope
F32 = jnp.float32
BF16 = jnp.bfloat16
T = 1024
H = 512
B = 128
W = 256
L = 128
K = 3

R = 96

DIRECT = 4

SHORT = 2

NEAR = (2, 1, 3)
ROW = [(d, e) for d in (2, 1, 3) for e in range(2)] + [(0, 1)]


def mod4(v):
    return lax.rem(v + 4, 4)


def row_sums(v):
    sq = v * v
    hi = sq.astype(BF16)
    lo = (sq - hi.astype(F32)).astype(BF16)
    ones = jnp.ones((8, v.shape[1]), BF16)
    dims = (((1,), (1,)), ((), ()))
    out = lax.dot_general(ones, hi, dims, preferred_element_type=F32)
    return out + lax.dot_general(ones, lo, dims, preferred_element_type=F32)


def as_columns(row):
    return jnp.transpose(jnp.broadcast_to(row[:1], (L, L)), (1, 0))


def kernel(
    tok_h, gain_h, wg_h, wu_h, wd_h, ogain_h, out,
    tok, gain, wg, wu, wd, ogain, xg, wb, wdb, part, zr, zs, rbuf, rdir, hall, begun, psend, p1, p2, s1, s2, p3, p4,
    sq_s, sq_r, sq2_r, st_s, st_r, st2_s, st2_r, st3_r,
    sent, head, loc, xa_rs, xb_rs, xc_rs, w_rs, f_rs, d_rs, df_rs, relay_rs, sum_rs, shown_rs, h_rs,
    p_rs, q_rs, t_rs, o_rs, of_rs,
):
    ra, cb = lax.axis_index("ra"), lax.axis_index("cb")
    z, y, x, c = ra // 4, lax.rem(ra, 4), cb // 2, lax.rem(cb, 2)

    def dev(dz=0, dy=0, dx=0, dc=0):
        return (mod4(z + dz) * 4 + mod4(y + dy), mod4(x + dx) * 2 + lax.rem(c + dc, 2))

    sends = []

    def send(src, dst, rs, to):
        cp = pltpu.make_async_remote_copy(
            src_ref=src, dst_ref=dst, send_sem=sent, recv_sem=rs, device_id=to, device_id_type=MESH
        )
        cp.start()
        sends.append(cp)
        return cp

    def arrived(ref, sem):
        pltpu.make_async_copy(ref, ref, sem).wait()

    def local(src, dst, sem):
        cp = pltpu.make_async_copy(src, dst, sem)
        cp.start()
        return cp

    partners = [dev(dy=d) for d in NEAR] + [dev(dz=d) for d in NEAR] + [dev(dx=d, dc=e) for d, e in ROW]
    bar = pltpu.get_barrier_semaphore()
    for p in partners:
        pl.semaphore_signal(bar, inc=1, device_id=p, device_id_type=MESH)

    heads = [
        local(src, dst, head.at[i])
        for i, (src, dst) in enumerate(
            ((tok_h, tok), (gain_h, gain), (wg_h, wg), (wu_h, wu), (wd_h, wd), (ogain_h, ogain))
        )
    ]

    def tile0(yy):
        return jnp.minimum(3 * yy, 8)

    def cols(yy, k):
        return pl.ds(pl.multiple_of((tile0(yy) + k) * L, L), L)

    def rows(start, size):
        return pl.ds(pl.multiple_of(start, 16), size)

    for k in range(K):
        local(wg_h.at[:, cols(y, k)], wb.at[k, c, 0, :, :L], loc.at[k])
        local(wu_h.at[:, cols(y, k)], wb.at[k, c, 0, :, L:], loc.at[k])
    local_d = local(wd_h.at[pl.ds(tile0(y), K)], wdb.at[y, :, c], loc.at[K])

    heads[0].wait()
    heads[1].wait()
    t32 = tok[rows(c * H, H), :].astype(F32)
    xg[0] = (t32 * gain[...]).astype(BF16)
    sq = row_sums(t32)
    for b in range(4):
        sq_s[b] = sq[:, b * L : (b + 1) * L]
    for h in heads[2:]:
        h.wait()
    with scope("barrier"):
        pl.semaphore_wait(bar, len(partners))

    quarter = rows(x * R, R)
    rest = slice(4 * R, H)
    xa = {d: send(xg.at[0, quarter], xg.at[d, quarter], xa_rs.at[d - 1], dev(dy=d)) for d in NEAR}
    for d in NEAR:
        send(xg.at[0, rest], xg.at[d, rest], xb_rs, dev(dy=d))
    for d in NEAR:
        send(sq_s, sq_r.at[d - 1], q_rs.at[0], dev(dy=d))
    for k in range(K):
        for d in NEAR:
            yy = mod4(y + d)
            send(wg.at[:, cols(yy, k)], wb.at[k, c, d, :, :L], w_rs.at[k, d - 1], dev(dy=d))
            send(wu.at[:, cols(yy, k)], wb.at[k, c, d, :, L:], w_rs.at[k, d - 1], dev(dy=d))
    for d in NEAR:
        send(wd.at[pl.ds(tile0(mod4(y + d)), K)], wdb.at[y, :, c], d_rs, dev(dy=d))
    for d in (1, 3, 2):
        with scope(f"wait_xa#d={d}"):
            xa[d].wait_recv()
        for e in NEAR:
            send(xg.at[d, quarter], xg.at[d, quarter], xc_rs, dev(dx=e))
    with scope("wait_xb"):
        arrived(xg.at[1:, rest], xb_rs)
    with scope("wait_sq"):
        arrived(sq_r, q_rs.at[0])
    for b in range(4):
        st2_s[b] = sq_s[b] + sq_r[0, b] + sq_r[1, b] + sq_r[2, b]
    for d in NEAR:
        send(st2_s.at[mod4(z + d)], sq2_r.at[d - 1], q_rs.at[1], dev(dz=d))

    own_rows = rows(z * B, B)
    h = B // 2
    up1, dn1 = dev(dz=1), dev(dz=3)

    def half(zz, i):
        return rows(mod4(z + zz) * B + i * h, h)

    def columns_of(k):
        with scope(f"wait_w#k={k}"):
            for d in (0,) + NEAR:
                arrived(wb.at[k, c, d], w_rs.at[k, d - 1] if d else loc.at[k])
                send(wb.at[k, c, d], wb.at[k, c, d], f_rs.at[k], dev(dc=1))

    relay, shown = {}, {}

    def multiply(u):
        k, cc = u // 2, lax.rem(c + u % 2, 2)
        if u % 2:
            with scope(f"wait_f#k={k}"):
                arrived(wb.at[k, cc], f_rs.at[k])
        acc = jnp.zeros((H, 2 * L), F32)
        for d in range(4):
            acc = acc + jnp.dot(xg[d], wb[k, cc, d], preferred_element_type=F32)
        part[u] = acc.astype(BF16)
        if u >= DIRECT:
            for d in NEAR:
                zz = rows(mod4(z + d) * B, B)
                send(part.at[u, zz], rdir.at[u - DIRECT, d - 1], sum_rs.at[u], dev(dz=d))
            return
        relay[u, 0] = send(part.at[u, half(2, 0)], zr.at[u, 0], relay_rs.at[u, 0], up1)
        relay[u, 1] = send(part.at[u, half(2, 1)], zr.at[u, 1], relay_rs.at[u, 1], dn1)
        send(part.at[u, half(1, 1)], rbuf.at[u, 0, h:], sum_rs.at[u], up1)
        send(part.at[u, half(3, 0)], rbuf.at[u, 1, :h], sum_rs.at[u], dn1)

    def add(u):
        with scope(f"wait_relay#u={u}"):
            relay[u, 0].wait_recv()
        zs[u, 0] = (part[u, half(1, 0), :].astype(F32) + zr[u, 0].astype(F32)).astype(BF16)
        send(zs.at[u, 0], rbuf.at[u, 0, :h], sum_rs.at[u], up1)
        relay[u, 1].wait_recv()
        zs[u, 1] = (part[u, half(3, 1), :].astype(F32) + zr[u, 1].astype(F32)).astype(BF16)
        send(zs.at[u, 1], rbuf.at[u, 1, h:], sum_rs.at[u], dn1)

    def lanes_of(u):
        return pl.ds(pl.multiple_of((u // 2 * 2 + lax.rem(c + u % 2, 2)) * L, L), L)

    def finish(u):
        with scope(f"wait_sum#u={u}"):
            arrived(rdir.at[u - DIRECT] if u >= DIRECT else rbuf.at[u], sum_rs.at[u])
        total = part[u, own_rows, :].astype(F32)
        for v in [rdir[u - DIRECT, d] for d in range(3)] if u >= DIRECT else [rbuf[u, d] for d in range(2)]:
            total = total + v.astype(F32)
        gate, up = total[:, :L] * inv, total[:, L:] * inv
        hid = gate / (1.0 + jnp.exp(-gate)) * up
        if u < 2:
            hid = jnp.where(y == 3, jnp.zeros_like(hid), hid)
        hall[own_rows, lanes_of(u)] = hid.astype(BF16)
        block = hall.at[own_rows, lanes_of(u)]
        if u >= SHORT:
            for d in NEAR:
                send(block, block, h_rs.at[u // DIRECT], dev(dz=d))
            return
        shown[u, 0] = send(block, block, shown_rs.at[u, 0], up1)
        shown[u, 1] = send(block, block, shown_rs.at[u, 1], dn1)

    def pass_on(u):
        with scope(f"wait_shown#u={u}"):
            shown[u, 0].wait_recv()
            block = hall.at[half(3, 0), lanes_of(u)]
            send(block, block, h_rs.at[0], up1)
            shown[u, 1].wait_recv()
            block = hall.at[half(1, 1), lanes_of(u)]
            send(block, block, h_rs.at[0], dn1)

    columns_of(0)
    with scope("wait_xc"):
        arrived(xg.at[1:, : 3 * R], xc_rs)
    multiply(0)
    with scope("wait_sq2"):
        arrived(sq2_r, q_rs.at[1])
    total = st2_s[z] + sq2_r[0] + sq2_r[1] + sq2_r[2]
    inv = as_columns(lax.rsqrt(total / D + EPS))
    multiply(1)
    add(0)
    add(1)
    columns_of(1)
    multiply(2)
    multiply(3)
    finish(0)
    finish(1)
    add(2)
    add(3)
    columns_of(2)
    multiply(4)
    multiply(5)
    pass_on(0)
    pass_on(1)
    finish(2)
    finish(3)
    finish(4)
    finish(5)
    with scope("wait_d"):
        local_d.wait()
        arrived(wdb.at[:3, :, c], d_rs)
        send(wdb.at[:, :, c], wdb.at[:, :, c], df_rs, dev(dc=1))
    with scope("wait_df"):
        arrived(wdb.at[:, :, c], df_rs)
    with scope("wait_h03"):
        arrived(hall.at[:, : 2 * L], h_rs.at[0])
    for yy in range(4):
        w = wdb[yy, :2].reshape(4 * L, W)
        begun[yy] = jnp.dot(hall[:, : 4 * L], w, preferred_element_type=F32)
    with scope("wait_h45"):
        arrived(hall.at[: 3 * B, 4 * L :], h_rs.at[1])

    for dy in (2, 1, 3, 0):
        yy = mod4(y + dy)
        acc = begun[yy] + jnp.dot(hall[:, 4 * L :], wdb[yy, 2].reshape(2 * L, W), preferred_element_type=F32)
        psend[yy] = acc.astype(BF16).reshape(4, 2, B // 2, W)
        if dy:
            send(psend.at[yy, :, 0], p1.at[dy - 1], p_rs.at[0], dev(dy=dy))
        for dx in NEAR:
            send(psend.at[yy, mod4(x + dx), 1], p2.at[dx - 1, yy], p_rs.at[1], dev(dx=dx))
    with scope("wait_p1"):
        arrived(p1, p_rs.at[0])
    for xx in range(4):
        v = psend[y, xx, 0].astype(F32)
        for d in range(3):
            v = v + p1[d, xx].astype(F32)
        s1[xx] = v.astype(BF16)
    for d in NEAR:
        send(s1.at[mod4(x + d)], p3.at[d - 1], p_rs.at[2], dev(dx=d))
    with scope("wait_p2"):
        arrived(p2, p_rs.at[1])
    for yy in range(4):
        v = psend[yy, x, 1].astype(F32)
        for d in range(3):
            v = v + p2[d, yy].astype(F32)
        s2[yy] = v.astype(BF16)
    for d in NEAR:
        send(s2.at[mod4(y + d)], p4.at[d - 1], p_rs.at[3], dev(dy=d))
    piece = c * H + x * B
    with scope("wait_p3"):
        arrived(p3, p_rs.at[2])
    v1 = s1[x].astype(F32)
    for d in range(3):
        v1 = v1 + p3[d].astype(F32)
    with scope("wait_p4"):
        arrived(p4, p_rs.at[3])
    v2 = s2[y].astype(F32)
    for d in range(3):
        v2 = v2 + p4[d].astype(F32)
    stream = 0.5 * tok[rows(piece, B), :].astype(F32) + jnp.concatenate([v1, v2], axis=0)
    out[rows(piece, B), :] = stream.astype(BF16)

    ag = {d: send(out.at[rows(piece, B), :], out.at[rows(piece, B), :], o_rs.at[d - 1], dev(dx=d)) for d in NEAR}
    st_s[...] = row_sums(stream)
    for d in NEAR:
        send(st_s, st_r.at[d - 1], t_rs.at[0], dev(dz=d))
    with scope("wait_st"):
        arrived(st_r, t_rs.at[0])
    st3_r[8] = st_s[...] + st_r[0] + st_r[1] + st_r[2]
    for d in NEAR:
        send(st3_r.at[8], st2_r.at[d - 1], t_rs.at[1], dev(dy=d))
    with scope("wait_o"):
        for d in (0,) + NEAR:
            if d:
                ag[d].wait_recv()
            block = out.at[rows(c * H + mod4(x - d) * B, B), :]
            send(block, block, of_rs, dev(dc=1))
    with scope("wait_st2"):
        arrived(st2_r, t_rs.at[1])
    st3_r[2 * x + c] = st3_r[8] + st2_r[0] + st2_r[1] + st2_r[2]
    me = st3_r.at[2 * x + c]
    for d, e in ROW:
        send(me, me, t_rs.at[2], dev(dx=d, dc=e))
    with scope("wait_of"):
        arrived(out.at[:H], of_rs)
    with scope("wait_st3"):
        arrived(st3_r.at[:7], t_rs.at[2])
    with scope("wait_sends"):
        for s in sends:
            s.wait_send()
    _n = scope("norm")
    _n.__enter__()
    for xx in range(4):
        for cc in range(2):
            factor = as_columns(lax.rsqrt(st3_r[2 * xx + cc] / D + EPS))
            r = slice(cc * H + xx * B, cc * H + (xx + 1) * B)
            for h in range(2):
                lanes = slice(h * L, (h + 1) * L)
                out[r, lanes] = (out[r, lanes].astype(F32) * factor * ogain[:, lanes]).astype(BF16)
    _n.__exit__(None, None, None)


def body(tokens, norm_gain, gate_weight, up_weight, down_weight, out_gain):
    dma = pltpu.SemaphoreType.DMA
    hbm = pl.BlockSpec(memory_space=pltpu.HBM)
    operands = (
        tokens,
        norm_gain.reshape(1, W),
        gate_weight,
        up_weight,
        down_weight.reshape(11, L, W),
        out_gain.reshape(1, W),
    )
    return pl.pallas_call(
        kernel,
        out_shape=jax.ShapeDtypeStruct((T, W), BF16),
        in_specs=[hbm] * 6,
        out_specs=pl.BlockSpec(memory_space=pltpu.VMEM),
        scratch_shapes=[
            pltpu.VMEM((T, W), BF16),
            pltpu.VMEM((1, W), F32),
            pltpu.VMEM((W, 11 * L), BF16),
            pltpu.VMEM((W, 11 * L), BF16),
            pltpu.VMEM((11, L, W), BF16),
            pltpu.VMEM((1, W), F32),
            pltpu.VMEM((4, H, W), BF16),
            pltpu.VMEM((K, 2, 4, W, 2 * L), BF16),
            pltpu.VMEM((4, K, 2, L, W), BF16),
            pltpu.VMEM((2 * K, H, 2 * L), BF16),
            pltpu.VMEM((2 * K, 2, B // 2, 2 * L), BF16),
            pltpu.VMEM((2 * K, 2, B // 2, 2 * L), BF16),
            pltpu.VMEM((2 * K, 2, B, 2 * L), BF16),
            pltpu.VMEM((2 * K - DIRECT, 3, B, 2 * L), BF16),
            pltpu.VMEM((H, 2 * K * L), BF16),
            pltpu.VMEM((4, H, W), F32),
            pltpu.VMEM((4, 4, 2, B // 2, W), BF16),
            pltpu.VMEM((3, 4, B // 2, W), BF16),
            pltpu.VMEM((3, 4, B // 2, W), BF16),
            pltpu.VMEM((4, B // 2, W), BF16),
            pltpu.VMEM((4, B // 2, W), BF16),
            pltpu.VMEM((3, B // 2, W), BF16),
            pltpu.VMEM((3, B // 2, W), BF16),
            pltpu.VMEM((4, 8, L), F32),
            pltpu.VMEM((3, 4, 8, L), F32),
            pltpu.VMEM((3, 8, L), F32),
            pltpu.VMEM((8, L), F32),
            pltpu.VMEM((3, 8, L), F32),
            pltpu.VMEM((4, 8, L), F32),
            pltpu.VMEM((3, 8, L), F32),
            pltpu.VMEM((9, 8, L), F32),
            dma,
            dma((6,)),
            dma((K + 1,)),
            dma((3,)), dma, dma,
            dma((K, 3)), dma((K,)), dma, dma,
            dma((DIRECT, 2)), dma((2 * K,)),
            dma((SHORT, 2)), dma((2,)),
            dma((4,)), dma((2,)), dma((3,)),
            dma((3,)), dma,
        ],
        compiler_params=pltpu.CompilerParams(
            collective_id=0, has_side_effects=True, vmem_limit_bytes=40 * 1024 * 1024
        ),
    )(*[pltpu.with_memory_space_constraint(a, pltpu.HBM) for a in operands])


def solution(mesh):
    placed = (P(None, "ra"), P("ra"), P("ra", "cb"), P("ra", "cb"), P("cb", "ra"), P("ra"))
    return jax.shard_map(body, mesh=mesh, in_specs=placed, out_specs=P(None, "ra"), check_vma=False)
```

time: 80.2 us -> 74 us (0.923)
  Pallas kernels: 79.3 us -> 73.1 us
    pallas_call x1, Pallas kernels: 79.3 us -> 73.1 us  [body(): pl.pallas_call(kernel, out_shape=jax.ShapeDtypeStruct((T, W), BF16), in_s...]
where the time goes in v3:
time: 74 us; the launch traced here: 73.9 us
  Pallas kernels  73.1 us (99%)
  local copies, waits for them, and re-layouts  0.8 us (1%)
    pallas_call x1, Pallas kernels, body(): pl.pallas_call(kernel, out_shape=jax.ShapeDtypeStruct((T, W), BF16), in_s...  73.1 us

profile of v3, /device:TPU:1, one launch (start us, length us, event | category | flops | bytes accessed | tf_op | source)
XLA Modules:
  0.0 73.9 jit_solution(11194887163403449216)
XLA Ops:
  0.0 73.1 %shard_map.64 = bf16[1024,256]{1,0:T(8,128)(2,1)S(1)} custom-call(bf16[1024,256]{1,0:T(8,128)(2,1)} %tok_h.1, f32[1,256]{1,0:T(1,128)} %bitcast.4, bf16[256,1408]{1,0:T(8,128)(2,1)} %wg_h.1, bf16[256,1408]{1,0:T(8,128)(2,1)} %wu_h.1, bf16[11,128,256]{2,1,0:T(8,128)(2,1)} %bitcast.3, f32[1,256]{1,0:T(1,128)} %bitcast.5), custom_call_target="tpu_custom_call" | custom-call | tf_op jit(solution)/shard_map/pallas_call | solution.py:354
  73.1 0.8 %copy.8 = bf16[1024,256]{1,0:T(8,128)(2,1)} copy(bf16[1024,256]{1,0:T(8,128)(2,1)S(1)} %shard_map.64) | data formatting | bytes 1048576

commit v4 on v3

v4 whole, which is shorter than its diff:
```python
import functools

import jax
import jax.numpy as jnp
from jax import lax
from jax.experimental import pallas as pl
from jax.experimental.pallas import tpu as pltpu
from jax.sharding import PartitionSpec as P

D = 4096
EPS = 1e-06
MESH = pl.DeviceIdType.MESH
scope = jax.named_scope
F32 = jnp.float32
BF16 = jnp.bfloat16
T = 1024
H = 512
B = 128
W = 256
L = 128
K = 3

R = 96

S0 = 64
HALVES = ((0, S0), (S0, B))

JOBS = (
    (0, 1, 0, B, True, True, 0),
    (1, 1, 0, B, True, True, 0),
    (2, 1, 0, B, True, False, 0),
    (3, 1, 0, B, True, False, 0),
    (4, 1, *HALVES[0], False, False, 1),
    (5, 1, *HALVES[0], False, False, 1),
    (4, 2, *HALVES[1], False, False, 2),
)

NEAR = (2, 1, 3)
PLANE = [(f, d, e) for f in (2, 1, 3, 0) for d in (2, 1, 3, 0) for e in (1, 0) if (f, d, e) != (0, 0, 0)]


def mod4(v):
    return lax.rem(v + 4, 4)


def row_sums(v):
    sq = v * v
    hi = sq.astype(BF16)
    lo = (sq - hi.astype(F32)).astype(BF16)
    ones = jnp.ones((8, v.shape[1]), BF16)
    dims = (((1,), (1,)), ((), ()))
    out = lax.dot_general(ones, hi, dims, preferred_element_type=F32)
    return (out + lax.dot_general(ones, lo, dims, preferred_element_type=F32))[:1]


def as_columns(row):
    return jnp.transpose(jnp.broadcast_to(row, (L, L)), (1, 0))


def kernel(
    tok_h, gain_h, wg_h, wu_h, wd_h, ogain_h, out,
    tok, gain, wg, wu, wd, ogain, xg, wb, wdb, part, zr, zs, rbuf, rdir, hall, begun, psend, p1, p2, s1, s2, p3, p4,
    sq_s, sq_r, sq2_r, st2_s, st_s, st_r, st_all, sq_n,
    sent, head, loc, xa_rs, xb_rs, xc_rs, w_rs, f_rs, d_rs, df_rs, relay_rs, sum_rs, shown_rs, h_rs,
    p_rs, q_rs, t_rs, o_rs, of_rs,
):
    ra, cb = lax.axis_index("ra"), lax.axis_index("cb")
    z, y, x, c = ra // 4, lax.rem(ra, 4), cb // 2, lax.rem(cb, 2)

    def dev(dz=0, dy=0, dx=0, dc=0):
        return (mod4(z + dz) * 4 + mod4(y + dy), mod4(x + dx) * 2 + lax.rem(c + dc, 2))

    sends = []

    def send(src, dst, rs, to):
        cp = pltpu.make_async_remote_copy(
            src_ref=src, dst_ref=dst, send_sem=sent, recv_sem=rs, device_id=to, device_id_type=MESH
        )
        cp.start()
        sends.append(cp)
        return cp

    def arrived(ref, sem):
        pltpu.make_async_copy(ref, ref, sem).wait()

    def local(src, dst, sem):
        cp = pltpu.make_async_copy(src, dst, sem)
        cp.start()
        return cp

    partners = [dev(dz=d) for d in NEAR] + [dev(dy=d) for d in NEAR] + [dev(dx=d) for d in NEAR] + [dev(dc=1)]
    bar = pltpu.get_barrier_semaphore()
    for p in partners:
        pl.semaphore_signal(bar, inc=1, device_id=p, device_id_type=MESH)

    heads = [
        local(src, dst, head.at[i])
        for i, (src, dst) in enumerate(
            ((tok_h, tok), (gain_h, gain), (wg_h, wg), (wu_h, wu), (wd_h, wd), (ogain_h, ogain))
        )
    ]

    def tile0(yy):
        return jnp.minimum(3 * yy, 8)

    def cols(yy, k):
        return pl.ds(pl.multiple_of((tile0(yy) + k) * L, L), L)

    def rows(start, size):
        return pl.ds(pl.multiple_of(start, 16), size)

    for k in range(K):
        local(wg_h.at[:, cols(y, k)], wb.at[k, c, 0, :, :L], loc.at[k])
        local(wu_h.at[:, cols(y, k)], wb.at[k, c, 0, :, L:], loc.at[k])
    local_d = local(wd_h.at[pl.ds(tile0(y), K)], wdb.at[y, :, c], loc.at[K])

    heads[0].wait()
    heads[1].wait()
    t32 = tok[rows(c * H, H), :].astype(F32)
    xg[0] = (t32 * gain[...]).astype(BF16)
    sq = row_sums(t32)
    for b in range(4):
        sq_s[b] = sq[:, b * L : (b + 1) * L]
    for h in heads[2:]:
        h.wait()
    with scope("barrier"):
        pl.semaphore_wait(bar, len(partners))

    quarter = rows(x * R, R)
    rest = slice(4 * R, H)
    xa = {d: send(xg.at[0, quarter], xg.at[d, quarter], xa_rs.at[d - 1], dev(dy=d)) for d in NEAR}
    for d in NEAR:
        send(xg.at[0, rest], xg.at[d, rest], xb_rs, dev(dy=d))
    for d in NEAR:
        send(sq_s, sq_r.at[d - 1], q_rs.at[0], dev(dy=d))
    for k in range(K):
        for d in NEAR:
            yy = mod4(y + d)
            send(wg.at[:, cols(yy, k)], wb.at[k, c, d, :, :L], w_rs.at[k, d - 1], dev(dy=d))
            send(wu.at[:, cols(yy, k)], wb.at[k, c, d, :, L:], w_rs.at[k, d - 1], dev(dy=d))
    for d in NEAR:
        send(wd.at[pl.ds(tile0(mod4(y + d)), K)], wdb.at[y, :, c], d_rs, dev(dy=d))
    for d in (1, 3, 2):
        with scope(f"wait_xa#d={d}"):
            xa[d].wait_recv()
        for e in NEAR:
            send(xg.at[d, quarter], xg.at[d, quarter], xc_rs, dev(dx=e))
    with scope("wait_xb"):
        arrived(xg.at[1:, rest], xb_rs)
    with scope("wait_sq"):
        arrived(sq_r, q_rs.at[0])
    for b in range(4):
        st2_s[b] = sq_s[b] + sq_r[0, b] + sq_r[1, b] + sq_r[2, b]
    for d in NEAR:
        send(st2_s.at[mod4(z + d)], sq2_r.at[d - 1], q_rs.at[1], dev(dz=d))

    up1, dn1 = dev(dz=1), dev(dz=3)

    def columns_of(k):
        with scope(f"wait_w#k={k}"):
            for d in (0,) + NEAR:
                arrived(wb.at[k, c, d], w_rs.at[k, d - 1] if d else loc.at[k])
                send(wb.at[k, c, d], wb.at[k, c, d], f_rs.at[k], dev(dc=1))

    def block_of(dz, r0, r1):
        return rows(mod4(z + dz) * B + r0, r1 - r0)

    def multiply(u):
        k, cc = u // 2, lax.rem(c + u % 2, 2)
        if u % 2:
            with scope(f"wait_f#k={k}"):
                arrived(wb.at[k, cc], f_rs.at[k])
        acc = jnp.zeros((H, 2 * L), F32)
        for d in range(4):
            acc = acc + jnp.dot(xg[d], wb[k, cc, d], preferred_element_type=F32)
        part[u] = acc.astype(BF16)

    def start(j):
        u, n, r0, r1, through, _, _ = JOBS[j]
        us, mid = slice(u, u + n), (r0 + r1) // 2
        if not through:
            for d in NEAR:
                send(part.at[us, block_of(d, r0, r1)], rdir.at[us, d - 1, r0:r1], sum_rs.at[j], dev(dz=d))
            return
        send(part.at[us, block_of(2, r0, mid)], zr.at[us, 0, r0:mid], relay_rs.at[j, 0], up1)
        send(part.at[us, block_of(2, mid, r1)], zr.at[us, 1, mid:r1], relay_rs.at[j, 1], dn1)
        send(part.at[us, block_of(1, mid, r1)], rbuf.at[us, 0, mid:r1], sum_rs.at[j], up1)
        send(part.at[us, block_of(3, r0, mid)], rbuf.at[us, 1, r0:mid], sum_rs.at[j], dn1)

    def add(j):
        u, n, r0, r1, _, _, _ = JOBS[j]
        us, mid = slice(u, u + n), (r0 + r1) // 2
        for side, to, dz, a, b in ((0, up1, 1, r0, mid), (1, dn1, 3, mid, r1)):
            with scope(f"wait_relay#j={j}"):
                arrived(zr.at[us, side, a:b], relay_rs.at[j, side])
            for v in range(u, u + n):
                mine = part[v, block_of(dz, a, b), :].astype(F32)
                zs[v, side, a:b] = (mine + zr[v, side, a:b].astype(F32)).astype(BF16)
            send(zs.at[us, side, a:b], rbuf.at[us, side, a:b], sum_rs.at[j], to)

    def lanes_of(u, n=1):
        if n == 2:
            return slice(u * L, (u + 2) * L)
        return pl.ds(pl.multiple_of((u // 2 * 2 + lax.rem(c + u % 2, 2)) * L, L), L)

    def finish(j):
        u, n, r0, r1, through, passing, group = JOBS[j]
        us = slice(u, u + n)
        came = rbuf if through else rdir
        with scope(f"wait_sum#j={j}"):
            arrived(came.at[us, :, r0:r1], sum_rs.at[j])
        for v in range(u, u + n):
            total = part[v, block_of(0, r0, r1), :].astype(F32)
            for d in range(2 if through else 3):
                total = total + came[v, d, r0:r1].astype(F32)
            gate, up = total[:, :L] * inv[r0:r1], total[:, L:] * inv[r0:r1]
            hid = gate / (1.0 + jnp.exp(-gate)) * up
            if v < 2:
                hid = jnp.where(y == 3, jnp.zeros_like(hid), hid)
            hall[z, r0:r1, lanes_of(v)] = hid.astype(BF16)
        block = hall.at[z, r0:r1, lanes_of(u, n)]
        if passing:
            send(block, block, shown_rs.at[j, 0], up1)
            send(block, block, shown_rs.at[j, 1], dn1)
        else:
            for d in NEAR:
                send(block, block, h_rs.at[group], dev(dz=d))

    def pass_on(j):
        u, n, r0, r1, _, _, group = JOBS[j]
        mid = (r0 + r1) // 2
        for side, to, dz, a, b in ((0, up1, 3, r0, mid), (1, dn1, 1, mid, r1)):
            with scope(f"wait_shown#j={j}"):
                arrived(hall.at[mod4(z + dz), r0:r1, lanes_of(u, n)], shown_rs.at[j, side])
            block = hall.at[mod4(z + dz), a:b, lanes_of(u, n)]
            send(block, block, h_rs.at[group], to)

    def all_hidden(group):
        tiles = sum((r1 - r0) * n * (1 if passing else 3) for _, n, r0, r1, _, passing, g in JOBS if g == group)
        with scope(f"wait_h#g={group}"):
            arrived(xg.at[:, : tiles // 8], h_rs.at[group])

    columns_of(0)
    with scope("wait_xc"):
        arrived(xg.at[1:, : 3 * R], xc_rs)
    multiply(0)
    start(0)
    with scope("wait_sq2"):
        arrived(sq2_r, q_rs.at[1])
    total = st2_s[z] + sq2_r[0] + sq2_r[1] + sq2_r[2]
    inv = as_columns(lax.rsqrt(total / D + EPS))
    multiply(1)
    start(1)
    add(0)
    add(1)
    columns_of(1)
    multiply(2)
    start(2)
    multiply(3)
    start(3)
    finish(0)
    finish(1)
    add(2)
    add(3)
    columns_of(2)
    multiply(4)
    start(4)
    multiply(5)
    start(5)
    start(6)
    pass_on(0)
    pass_on(1)
    finish(2)
    finish(3)
    finish(4)
    finish(5)
    with scope("wait_d"):
        local_d.wait()
        arrived(wdb.at[:3, :, c], d_rs)
        send(wdb.at[:, :, c], wdb.at[:, :, c], df_rs, dev(dc=1))
    finish(6)
    with scope("wait_df"):
        arrived(wdb.at[:, :, c], df_rs)

    all_hidden(0)
    for yy in range(4):
        w = wdb[yy, :2].reshape(4 * L, W)
        begun[yy] = jnp.dot(hall[:, :, : 4 * L].reshape(H, 4 * L), w, preferred_element_type=F32).reshape(4, B, W)
    for i, (r0, r1) in enumerate(HALVES):
        all_hidden(1 + i)
        mid = (r0 + r1) // 2
        a, b = slice(r0, mid), slice(mid, r1)
        for dy in (2, 1, 3, 0):
            yy = mod4(y + dy)
            hid = hall[:, r0:r1, 4 * L :].reshape(4 * (r1 - r0), 2 * L)
            acc = jnp.dot(hid, wdb[yy, 2].reshape(2 * L, W), preferred_element_type=F32)
            psend[yy, :, r0:r1] = (begun[yy, :, r0:r1] + acc.reshape(4, r1 - r0, W)).astype(BF16)
            if dy:
                send(psend.at[yy, :, a], p1.at[dy - 1, :, a], p_rs.at[i, 0], dev(dy=dy))
            for dx in NEAR:
                send(psend.at[yy, mod4(x + dx), b], p2.at[dx - 1, yy, b], p_rs.at[i, 1], dev(dx=dx))
    for i, (r0, r1) in enumerate(HALVES):
        mid = (r0 + r1) // 2
        a, b = slice(r0, mid), slice(mid, r1)
        with scope(f"wait_p1#i={i}"):
            arrived(p1.at[:, :, a], p_rs.at[i, 0])
        for xx in range(4):
            v = psend[y, xx, a].astype(F32)
            for d in range(3):
                v = v + p1[d, xx, a].astype(F32)
            s1[xx, a] = v.astype(BF16)
        for d in NEAR:
            send(s1.at[mod4(x + d), a], p3.at[d - 1, a], p_rs.at[i, 2], dev(dx=d))
        with scope(f"wait_p2#i={i}"):
            arrived(p2.at[:, :, b], p_rs.at[i, 1])
        for yy in range(4):
            v = psend[yy, x, b].astype(F32)
            for d in range(3):
                v = v + p2[d, yy, b].astype(F32)
            s2[yy, b] = v.astype(BF16)
        for d in NEAR:
            send(s2.at[mod4(y + d), b], p4.at[d - 1, b], p_rs.at[i, 3], dev(dy=d))
    pieces = []
    for i, (r0, r1) in enumerate(HALVES):
        mid = (r0 + r1) // 2
        a, b = slice(r0, mid), slice(mid, r1)
        with scope(f"wait_p3#i={i}"):
            arrived(p3.at[:, a], p_rs.at[i, 2])
        v = s1[x, a].astype(F32)
        for d in range(3):
            v = v + p3[d, a].astype(F32)
        pieces.append(v)
        with scope(f"wait_p4#i={i}"):
            arrived(p4.at[:, b], p_rs.at[i, 3])
        v = s2[y, b].astype(F32)
        for d in range(3):
            v = v + p4[d, b].astype(F32)
        pieces.append(v)
    piece = rows(c * H + x * B, B)
    stream = 0.5 * tok[piece, :].astype(F32) + jnp.concatenate(pieces, axis=0)
    out[piece, :] = stream.astype(BF16)

    st_s[...] = row_sums(stream)
    for d in NEAR:
        send(st_s, st_r.at[d - 1], t_rs.at[0], dev(dz=d))
    ag = {d: send(out.at[piece, :], out.at[piece, :], o_rs.at[d - 1], dev(dx=d)) for d in NEAR}
    with scope("wait_st"):
        arrived(st_r, t_rs.at[0])
    mine = 2 * x + c
    st_all[mine, 0] = st_s[...] + st_r[0] + st_r[1] + st_r[2]
    for f, d, e in PLANE:
        send(st_all.at[mine, 0], st_all.at[mine, f], t_rs.at[1], dev(dy=f, dx=d, dc=e))
    with scope("wait_o"):
        for d in (0,) + NEAR:
            if d:
                ag[d].wait_recv()
            block = out.at[rows(c * H + mod4(x - d) * B, B), :]
            send(block, block, of_rs, dev(dc=1))
    with scope("wait_of"):
        arrived(out.at[:H], of_rs)
    with scope("wait_st2"):
        arrived(sq_n.at[: len(PLANE)], t_rs.at[1])
    with scope("wait_sends"):
        for s in sends:
            s.wait_send()
    for xx in range(4):
        for cc in range(2):
            total = st_all[2 * xx + cc, 0] + st_all[2 * xx + cc, 1] + st_all[2 * xx + cc, 2] + st_all[2 * xx + cc, 3]
            factor = as_columns(lax.rsqrt(total / D + EPS))
            r = slice(cc * H + xx * B, cc * H + (xx + 1) * B)
            for h in range(2):
                lanes = slice(h * L, (h + 1) * L)
                out[r, lanes] = (out[r, lanes].astype(F32) * factor * ogain[:, lanes]).astype(BF16)


def body(tokens, norm_gain, gate_weight, up_weight, down_weight, out_gain):
    dma = pltpu.SemaphoreType.DMA
    hbm = pl.BlockSpec(memory_space=pltpu.HBM)
    operands = (
        tokens,
        norm_gain.reshape(1, W),
        gate_weight,
        up_weight,
        down_weight.reshape(11, L, W),
        out_gain.reshape(1, W),
    )
    return pl.pallas_call(
        kernel,
        out_shape=jax.ShapeDtypeStruct((T, W), BF16),
        in_specs=[hbm] * 6,
        out_specs=pl.BlockSpec(memory_space=pltpu.VMEM),
        scratch_shapes=[
            pltpu.VMEM((T, W), BF16),
            pltpu.VMEM((1, W), F32),
            pltpu.VMEM((W, 11 * L), BF16),
            pltpu.VMEM((W, 11 * L), BF16),
            pltpu.VMEM((11, L, W), BF16),
            pltpu.VMEM((1, W), F32),
            pltpu.VMEM((4, H, W), BF16),
            pltpu.VMEM((K, 2, 4, W, 2 * L), BF16),
            pltpu.VMEM((4, K, 2, L, W), BF16),
            pltpu.VMEM((2 * K, H, 2 * L), BF16),
            pltpu.VMEM((2 * K, 2, B, 2 * L), BF16),
            pltpu.VMEM((2 * K, 2, B, 2 * L), BF16),
            pltpu.VMEM((2 * K, 2, B, 2 * L), BF16),
            pltpu.VMEM((2 * K, 3, B, 2 * L), BF16),
            pltpu.VMEM((4, B, 2 * K * L), BF16),
            pltpu.VMEM((4, 4, B, W), F32),
            pltpu.VMEM((4, 4, B, W), BF16),
            pltpu.VMEM((3, 4, B, W), BF16),
            pltpu.VMEM((3, 4, B, W), BF16),
            pltpu.VMEM((4, B, W), BF16),
            pltpu.VMEM((4, B, W), BF16),
            pltpu.VMEM((3, B, W), BF16),
            pltpu.VMEM((3, B, W), BF16),
            pltpu.VMEM((4, 1, L), F32),
            pltpu.VMEM((3, 4, 1, L), F32),
            pltpu.VMEM((3, 1, L), F32),
            pltpu.VMEM((4, 1, L), F32),
            pltpu.VMEM((1, L), F32),
            pltpu.VMEM((3, 1, L), F32),
            pltpu.VMEM((8, 4, 1, L), F32),
            pltpu.VMEM((32, 1, L), F32),
            dma,
            dma((6,)),
            dma((K + 1,)),
            dma((3,)), dma, dma,
            dma((K, 3)), dma((K,)), dma, dma,
            dma((len(JOBS), 2)), dma((len(JOBS),)),
            dma((len(JOBS), 2)), dma((3,)),
            dma((2, 4)), dma((2,)), dma((2,)),
            dma((3,)), dma,
        ],
        compiler_params=pltpu.CompilerParams(
            collective_id=0, has_side_effects=True, vmem_limit_bytes=40 * 1024 * 1024
        ),
    )(*[pltpu.with_memory_space_constraint(a, pltpu.HBM) for a in operands])


def solution(mesh):
    placed = (P(None, "ra"), P("ra"), P("ra", "cb"), P("ra", "cb"), P("cb", "ra"), P("ra"))
    return jax.shard_map(body, mesh=mesh, in_specs=placed, out_specs=P(None, "ra"), check_vma=False)
```

time: 74 us -> 71.1 us (0.961)
  Pallas kernels: 73.1 us -> 70.2 us
    pallas_call x1, Pallas kernels: 73.1 us -> 70.2 us  [body(): pl.pallas_call(kernel, out_shape=jax.ShapeDtypeStruct((T, W), BF16), in_s...]
where the time goes in v4:
time: 71.1 us; the launch traced here: 71 us
  Pallas kernels  70.2 us (99%)
  local copies, waits for them, and re-layouts  0.8 us (1%)
    pallas_call x1, Pallas kernels, body(): pl.pallas_call(kernel, out_shape=jax.ShapeDtypeStruct((T, W), BF16), in_s...  70.2 us

profile of v4, /device:TPU:1, one launch (start us, length us, event | category | flops | bytes accessed | tf_op | source)
XLA Modules:
  0.0 71.0 jit_solution(16278096873355935405)
XLA Ops:
  0.0 70.2 %shard_map.64 = bf16[1024,256]{1,0:T(8,128)(2,1)S(1)} custom-call(bf16[1024,256]{1,0:T(8,128)(2,1)} %tok_h.1, f32[1,256]{1,0:T(1,128)} %bitcast.4, bf16[256,1408]{1,0:T(8,128)(2,1)} %wg_h.1, bf16[256,1408]{1,0:T(8,128)(2,1)} %wu_h.1, bf16[11,128,256]{2,1,0:T(8,128)(2,1)} %bitcast.3, f32[1,256]{1,0:T(1,128)} %bitcast.5), custom_call_target="tpu_custom_call" | custom-call | tf_op jit(solution)/shard_map/pallas_call | solution.py:387
  70.2 0.8 %copy.8 = bf16[1024,256]{1,0:T(8,128)(2,1)} copy(bf16[1024,256]{1,0:T(8,128)(2,1)S(1)} %shard_map.64) | data formatting | bytes 1048576

commit v5 on v4

--- a/solution.py
+++ b/solution.py
@@ -25,15 +25,7 @@
 S0 = 64
 HALVES = ((0, S0), (S0, B))
 
-JOBS = (
-    (0, 1, 0, B, True, True, 0),
-    (1, 1, 0, B, True, True, 0),
-    (2, 1, 0, B, True, False, 0),
-    (3, 1, 0, B, True, False, 0),
-    (4, 1, *HALVES[0], False, False, 1),
-    (5, 1, *HALVES[0], False, False, 1),
-    (4, 2, *HALVES[1], False, False, 2),
-)
+JOBS = ((0, "z", False), (1, "z", False), (2, "z", True), (3, "z", True), (4, "y", False), (5, "y", False))
 
 NEAR = (2, 1, 3)
 PLANE = [(f, d, e) for f in (2, 1, 3, 0) for d in (2, 1, 3, 0) for e in (1, 0) if (f, d, e) != (0, 0, 0)]
@@ -59,9 +51,9 @@
 
 def kernel(
     tok_h, gain_h, wg_h, wu_h, wd_h, ogain_h, out,
-    tok, gain, wg, wu, wd, ogain, xg, wb, wdb, part, zr, zs, rbuf, rdir, hall, begun, psend, p1, p2, s1, s2, p3, p4,
-    sq_s, sq_r, sq2_r, st2_s, st_s, st_r, st_all, sq_n,
-    sent, head, loc, xa_rs, xb_rs, xc_rs, w_rs, f_rs, d_rs, df_rs, relay_rs, sum_rs, shown_rs, h_rs,
+    tok, gain, wg, wu, wd, ogain, xg, xz, wb, wdb, part, zr, zs, rbuf, rdir, hall, hz, begun, psend, p1, p2, s1, s2, p3, p4,
+    sq_s, sq_r, sq2_r, sq3_r, st2_s, st_s, st_r, st_all, sq_n,
+    sent, head, loc, xa_rs, xb_rs, xc_rs, xz_rs, w_rs, f_rs, d_rs, df_rs, relay_rs, sum_rs, h_rs, hy_rs,
     p_rs, q_rs, t_rs, o_rs, of_rs,
 ):
     ra, cb = lax.axis_index("ra"), lax.axis_index("cb")
@@ -110,8 +102,9 @@
         return pl.ds(pl.multiple_of(start, 16), size)
 
     for k in range(K):
-        local(wg_h.at[:, cols(y, k)], wb.at[k, c, 0, :, :L], loc.at[k])
-        local(wu_h.at[:, cols(y, k)], wb.at[k, c, 0, :, L:], loc.at[k])
+        own = cols(y if k < 2 else z, k)
+        local(wg_h.at[:, own], wb.at[k, c, 0, :, :L], loc.at[k])
+        local(wu_h.at[:, own], wb.at[k, c, 0, :, L:], loc.at[k])
     local_d = local(wd_h.at[pl.ds(tile0(y), K)], wdb.at[y, :, c], loc.at[K])
 
     heads[0].wait()
@@ -133,13 +126,12 @@
         send(xg.at[0, rest], xg.at[d, rest], xb_rs, dev(dy=d))
     for d in NEAR:
         send(sq_s, sq_r.at[d - 1], q_rs.at[0], dev(dy=d))
+    near_z = {d: send(xg.at[0], xz.at[d - 1], xz_rs.at[d - 1], dev(dz=d)) for d in (1, 3)}
     for k in range(K):
         for d in NEAR:
-            yy = mod4(y + d)
-            send(wg.at[:, cols(yy, k)], wb.at[k, c, d, :, :L], w_rs.at[k, d - 1], dev(dy=d))
-            send(wu.at[:, cols(yy, k)], wb.at[k, c, d, :, L:], w_rs.at[k, d - 1], dev(dy=d))
-    for d in NEAR:
-        send(wd.at[pl.ds(tile0(mod4(y + d)), K)], wdb.at[y, :, c], d_rs, dev(dy=d))
+            own, to = (mod4(y + d), dev(dy=d)) if k < 2 else (mod4(z + d), dev(dz=d))
+            send(wg.at[:, cols(own, k)], wb.at[k, c, d, :, :L], w_rs.at[k, d - 1], to)
+            send(wu.at[:, cols(own, k)], wb.at[k, c, d, :, L:], w_rs.at[k, d - 1], to)
     for d in (1, 3, 2):
         with scope(f"wait_xa#d={d}"):
             xa[d].wait_recv()
@@ -153,8 +145,11 @@
         st2_s[b] = sq_s[b] + sq_r[0, b] + sq_r[1, b] + sq_r[2, b]
     for d in NEAR:
         send(st2_s.at[mod4(z + d)], sq2_r.at[d - 1], q_rs.at[1], dev(dz=d))
-
-    up1, dn1 = dev(dz=1), dev(dz=3)
+        send(st2_s.at[y], sq3_r.at[d - 1], q_rs.at[2], dev(dz=d))
+    with scope("wait_xz"):
+        for d, to, half in ((1, 1, slice(0, H // 2)), (3, 3, slice(H // 2, H))):
+            near_z[d].wait_recv()
+            send(xz.at[d - 1, half], xz.at[1, half], xz_rs.at[1], dev(dz=to))
 
     def columns_of(k):
         with scope(f"wait_w#k={k}"):
@@ -162,8 +157,11 @@
                 arrived(wb.at[k, c, d], w_rs.at[k, d - 1] if d else loc.at[k])
                 send(wb.at[k, c, d], wb.at[k, c, d], f_rs.at[k], dev(dc=1))
 
-    def block_of(dz, r0, r1):
-        return rows(mod4(z + dz) * B + r0, r1 - r0)
+    def along(axis, d):
+        return (dev(dz=d), mod4(z + d)) if axis == "z" else (dev(dy=d), mod4(y + d))
+
+    def block_of(at, r0=0, r1=B):
+        return rows(at * B + r0, r1 - r0)
 
     def multiply(u):
         k, cc = u // 2, lax.rem(c + u % 2, 2)
@@ -172,73 +170,61 @@
                 arrived(wb.at[k, cc], f_rs.at[k])
         acc = jnp.zeros((H, 2 * L), F32)
         for d in range(4):
-            acc = acc + jnp.dot(xg[d], wb[k, cc, d], preferred_element_type=F32)
+            xs = xz[d - 1] if u >= 4 and d else xg[d]
+            acc = acc + jnp.dot(xs, wb[k, cc, d], preferred_element_type=F32)
         part[u] = acc.astype(BF16)
 
-    def start(j):
-        u, n, r0, r1, through, _, _ = JOBS[j]
-        us, mid = slice(u, u + n), (r0 + r1) // 2
+    half = B // 2
+
+    def start(u):
+        _, axis, through = JOBS[u]
         if not through:
             for d in NEAR:
-                send(part.at[us, block_of(d, r0, r1)], rdir.at[us, d - 1, r0:r1], sum_rs.at[j], dev(dz=d))
+                to, at = along(axis, d)
+                send(part.at[u, block_of(at)], rdir.at[u, d - 1], sum_rs.at[u], to)
             return
-        send(part.at[us, block_of(2, r0, mid)], zr.at[us, 0, r0:mid], relay_rs.at[j, 0], up1)
-        send(part.at[us, block_of(2, mid, r1)], zr.at[us, 1, mid:r1], relay_rs.at[j, 1], dn1)
-        send(part.at[us, block_of(1, mid, r1)], rbuf.at[us, 0, mid:r1], sum_rs.at[j], up1)
-        send(part.at[us, block_of(3, r0, mid)], rbuf.at[us, 1, r0:mid], sum_rs.at[j], dn1)
-
-    def add(j):
-        u, n, r0, r1, _, _, _ = JOBS[j]
-        us, mid = slice(u, u + n), (r0 + r1) // 2
-        for side, to, dz, a, b in ((0, up1, 1, r0, mid), (1, dn1, 3, mid, r1)):
-            with scope(f"wait_relay#j={j}"):
-                arrived(zr.at[us, side, a:b], relay_rs.at[j, side])
-            for v in range(u, u + n):
-                mine = part[v, block_of(dz, a, b), :].astype(F32)
-                zs[v, side, a:b] = (mine + zr[v, side, a:b].astype(F32)).astype(BF16)
-            send(zs.at[us, side, a:b], rbuf.at[us, side, a:b], sum_rs.at[j], to)
-
-    def lanes_of(u, n=1):
-        if n == 2:
-            return slice(u * L, (u + 2) * L)
-        return pl.ds(pl.multiple_of((u // 2 * 2 + lax.rem(c + u % 2, 2)) * L, L), L)
-
-    def finish(j):
-        u, n, r0, r1, through, passing, group = JOBS[j]
-        us = slice(u, u + n)
+        far = along(axis, 2)[1]
+        (up1, above), (dn1, below) = along(axis, 1), along(axis, 3)
+        send(part.at[u, block_of(far, 0, half)], zr.at[u, 0], relay_rs.at[u, 0], up1)
+        send(part.at[u, block_of(far, half, B)], zr.at[u, 1], relay_rs.at[u, 1], dn1)
+        send(part.at[u, block_of(above, half, B)], rbuf.at[u, 0, half:], sum_rs.at[u], up1)
+        send(part.at[u, block_of(below, 0, half)], rbuf.at[u, 1, :half], sum_rs.at[u], dn1)
+
+    def add(u):
+        _, axis, _ = JOBS[u]
+        for side, d, a, b in ((0, 1, 0, half), (1, 3, half, B)):
+            to, at = along(axis, d)
+            with scope(f"wait_relay#u={u}"):
+                arrived(zr.at[u, side], relay_rs.at[u, side])
+            zs[u, side] = (part[u, block_of(at, a, b), :].astype(F32) + zr[u, side].astype(F32)).astype(BF16)
+            send(zs.at[u, side], rbuf.at[u, side, a:b], sum_rs.at[u], to)
+
+    def core_of(u):
+        return lax.rem(c + u % 2, 2)
+
+    def finish(u):
+        _, axis, through = JOBS[u]
         came = rbuf if through else rdir
-        with scope(f"wait_sum#j={j}"):
-            arrived(came.at[us, :, r0:r1], sum_rs.at[j])
-        for v in range(u, u + n):
-            total = part[v, block_of(0, r0, r1), :].astype(F32)
-            for d in range(2 if through else 3):
-                total = total + came[v, d, r0:r1].astype(F32)
-            gate, up = total[:, :L] * inv[r0:r1], total[:, L:] * inv[r0:r1]
-            hid = gate / (1.0 + jnp.exp(-gate)) * up
-            if v < 2:
-                hid = jnp.where(y == 3, jnp.zeros_like(hid), hid)
-            hall[z, r0:r1, lanes_of(v)] = hid.astype(BF16)
-        block = hall.at[z, r0:r1, lanes_of(u, n)]
-        if passing:
-            send(block, block, shown_rs.at[j, 0], up1)
-            send(block, block, shown_rs.at[j, 1], dn1)
+        with scope(f"wait_sum#u={u}"):
+            arrived(came.at[u], sum_rs.at[u])
+        total = part[u, block_of(along(axis, 0)[1]), :].astype(F32)
+        for d in range(2 if through else 3):
+            total = total + came[u, d].astype(F32)
+        scale = inv if axis == "z" else inv_y
+        gate, up = total[:, :L] * scale, total[:, L:] * scale
+        hid = gate / (1.0 + jnp.exp(-gate)) * up
+        if u < 2:
+            hid = jnp.where(y == 3, jnp.zeros_like(hid), hid)
+        if axis == "z":
+            lanes = pl.ds(pl.multiple_of((u // 2 * 2 + core_of(u)) * L, L), L)
+            hall[z, :, lanes] = hid.astype(BF16)
+            block = hall.at[z, :, lanes]
         else:
-            for d in NEAR:
-                send(block, block, h_rs.at[group], dev(dz=d))
-
-    def pass_on(j):
-        u, n, r0, r1, _, _, group = JOBS[j]
-        mid = (r0 + r1) // 2
-        for side, to, dz, a, b in ((0, up1, 3, r0, mid), (1, dn1, 1, mid, r1)):
-            with scope(f"wait_shown#j={j}"):
-                arrived(hall.at[mod4(z + dz), r0:r1, lanes_of(u, n)], shown_rs.at[j, side])
-            block = hall.at[mod4(z + dz), a:b, lanes_of(u, n)]
-            send(block, block, h_rs.at[group], to)
-
-    def all_hidden(group):
-        tiles = sum((r1 - r0) * n * (1 if passing else 3) for _, n, r0, r1, _, passing, g in JOBS if g == group)
-        with scope(f"wait_h#g={group}"):
-            arrived(xg.at[:, : tiles // 8], h_rs.at[group])
+            lanes = pl.ds(pl.multiple_of(core_of(u) * L, L), L)
+            hz[z, :, lanes] = hid.astype(BF16)
+            block = hz.at[z, :, lanes]
+        for d in NEAR:
+            send(block, block, h_rs.at[u // 4], dev(dz=d))
 
     columns_of(0)
     with scope("wait_xc"):
@@ -247,47 +233,59 @@
     start(0)
     with scope("wait_sq2"):
         arrived(sq2_r, q_rs.at[1])
-    total = st2_s[z] + sq2_r[0] + sq2_r[1] + sq2_r[2]
-    inv = as_columns(lax.rsqrt(total / D + EPS))
+        arrived(sq3_r, q_rs.at[2])
+    inv = as_columns(lax.rsqrt((st2_s[z] + sq2_r[0] + sq2_r[1] + sq2_r[2]) / D + EPS))
+    inv_y = as_columns(lax.rsqrt((st2_s[y] + sq3_r[0] + sq3_r[1] + sq3_r[2]) / D + EPS))
     multiply(1)
     start(1)
-    add(0)
-    add(1)
-    columns_of(1)
-    multiply(2)
-    start(2)
-    multiply(3)
-    start(3)
-    finish(0)
-    finish(1)
-    add(2)
-    add(3)
     columns_of(2)
+    with scope("wait_xz2"):
+        arrived(xz.at[1], xz_rs.at[1])
     multiply(4)
     start(4)
     multiply(5)
     start(5)
-    start(6)
-    pass_on(0)
-    pass_on(1)
+    for d in NEAR:
+        send(wd.at[pl.ds(tile0(mod4(y + d)), K)], wdb.at[y, :, c], d_rs.at[d - 1], dev(dy=d))
+    columns_of(1)
+    multiply(2)
+    start(2)
+    finish(0)
+    multiply(3)
+    start(3)
+    finish(1)
+    add(2)
+    finish(4)
+    add(3)
+    finish(5)
     finish(2)
     finish(3)
-    finish(4)
-    finish(5)
+    with scope("wait_hz"):
+        arrived(hz.at[:3], h_rs.at[1])
+    last = slice(4 * L, 6 * L)
+    for i, (r0, r1) in enumerate(HALVES):
+        for d in NEAR:
+            send(hz.at[mod4(y + d), r0:r1], hall.at[y, r0:r1, last], hy_rs.at[i], dev(dy=d))
+    hall[y, :, last] = hz[y]
     with scope("wait_d"):
-        local_d.wait()
-        arrived(wdb.at[:3, :, c], d_rs)
-        send(wdb.at[:, :, c], wdb.at[:, :, c], df_rs, dev(dc=1))
-    finish(6)
+        for d in (0, 1, 3, 2):
+            if d:
+                arrived(wdb.at[0, :, c], d_rs.at[d - 1])
+            else:
+                local_d.wait()
+            block = wdb.at[mod4(y - d), :, c]
+            send(block, block, df_rs, dev(dc=1))
     with scope("wait_df"):
         arrived(wdb.at[:, :, c], df_rs)
 
-    all_hidden(0)
+    with scope("wait_h"):
+        arrived(hall.at[:3, :, : 4 * L], h_rs.at[0])
     for yy in range(4):
         w = wdb[yy, :2].reshape(4 * L, W)
         begun[yy] = jnp.dot(hall[:, :, : 4 * L].reshape(H, 4 * L), w, preferred_element_type=F32).reshape(4, B, W)
     for i, (r0, r1) in enumerate(HALVES):
-        all_hidden(1 + i)
+        with scope(f"wait_hy#i={i}"):
+            arrived(hall.at[:3, r0:r1, last], hy_rs.at[i])
         mid = (r0 + r1) // 2
         a, b = slice(r0, mid), slice(mid, r1)
         for dy in (2, 1, 3, 0):
@@ -397,14 +395,16 @@
             pltpu.VMEM((11, L, W), BF16),
             pltpu.VMEM((1, W), F32),
             pltpu.VMEM((4, H, W), BF16),
+            pltpu.VMEM((3, H, W), BF16),
             pltpu.VMEM((K, 2, 4, W, 2 * L), BF16),
             pltpu.VMEM((4, K, 2, L, W), BF16),
             pltpu.VMEM((2 * K, H, 2 * L), BF16),
-            pltpu.VMEM((2 * K, 2, B, 2 * L), BF16),
-            pltpu.VMEM((2 * K, 2, B, 2 * L), BF16),
+            pltpu.VMEM((2 * K, 2, B // 2, 2 * L), BF16),
+            pltpu.VMEM((2 * K, 2, B // 2, 2 * L), BF16),
             pltpu.VMEM((2 * K, 2, B, 2 * L), BF16),
             pltpu.VMEM((2 * K, 3, B, 2 * L), BF16),
             pltpu.VMEM((4, B, 2 * K * L), BF16),
+            pltpu.VMEM((4, B, 2 * L), BF16),
             pltpu.VMEM((4, 4, B, W), F32),
             pltpu.VMEM((4, 4, B, W), BF16),
             pltpu.VMEM((3, 4, B, W), BF16),
@@ -416,6 +416,7 @@
             pltpu.VMEM((4, 1, L), F32),
             pltpu.VMEM((3, 4, 1, L), F32),
             pltpu.VMEM((3, 1, L), F32),
+            pltpu.VMEM((3, 1, L), F32),
             pltpu.VMEM((4, 1, L), F32),
             pltpu.VMEM((1, L), F32),
             pltpu.VMEM((3, 1, L), F32),
@@ -424,11 +425,11 @@
             dma,
             dma((6,)),
             dma((K + 1,)),
-            dma((3,)), dma, dma,
-            dma((K, 3)), dma((K,)), dma, dma,
+            dma((3,)), dma, dma, dma((3,)),
+            dma((K, 3)), dma((K,)), dma((3,)), dma,
             dma((len(JOBS), 2)), dma((len(JOBS),)),
-            dma((len(JOBS), 2)), dma((3,)),
-            dma((2, 4)), dma((2,)), dma((2,)),
+            dma((2,)), dma((2,)),
+            dma((2, 4)), dma((3,)), dma((2,)),
             dma((3,)), dma,
         ],
         compiler_params=pltpu.CompilerParams(

time: 71.1 us -> 66.6 us (0.937)
  Pallas kernels: 70.2 us -> 65.7 us
    pallas_call x1, Pallas kernels: 70.2 us -> 65.7 us  [body(): pl.pallas_call(kernel, out_shape=jax.ShapeDtypeStruct((T, W), BF16), in_s...]
where the time goes in v5:
time: 66.6 us; the launch traced here: 66.5 us
  Pallas kernels  65.7 us (99%)
  local copies, waits for them, and re-layouts  0.8 us (1%)
    pallas_call x1, Pallas kernels, body(): pl.pallas_call(kernel, out_shape=jax.ShapeDtypeStruct((T, W), BF16), in_s...  65.7 us

profile of v5, /device:TPU:1, one launch (start us, length us, event | category | flops | bytes accessed | tf_op | source)
XLA Modules:
  0.0 66.5 jit_solution(2053314636344174929)
XLA Ops:
  0.0 65.7 %shard_map.64 = bf16[1024,256]{1,0:T(8,128)(2,1)S(1)} custom-call(bf16[1024,256]{1,0:T(8,128)(2,1)} %tok_h.1, f32[1,256]{1,0:T(1,128)} %bitcast.4, bf16[256,1408]{1,0:T(8,128)(2,1)} %wg_h.1, bf16[256,1408]{1,0:T(8,128)(2,1)} %wu_h.1, bf16[11,128,256]{2,1,0:T(8,128)(2,1)} %bitcast.3, f32[1,256]{1,0:T(1,128)} %bitcast.5), custom_call_target="tpu_custom_call" | custom-call | tf_op jit(solution)/shard_map/pallas_call | solution.py:385
  65.7 0.8 %copy.8 = bf16[1024,256]{1,0:T(8,128)(2,1)} copy(bf16[1024,256]{1,0:T(8,128)(2,1)S(1)} %shard_map.64) | data formatting | bytes 1048576

commit v6 on v5

--- a/solution.py
+++ b/solution.py
@@ -28,7 +28,8 @@
 JOBS = ((0, "z", False), (1, "z", False), (2, "z", True), (3, "z", True), (4, "y", False), (5, "y", False))
 
 NEAR = (2, 1, 3)
-PLANE = [(f, d, e) for f in (2, 1, 3, 0) for d in (2, 1, 3, 0) for e in (1, 0) if (f, d, e) != (0, 0, 0)]
+EVERYONE = [(g, f, d, e) for g in range(4) for f in range(4) for d in range(4) for e in range(2)][1:]
+EVERYONE.sort(key=lambda s: -sum(min(v, 4 - v) for v in s[:3]))
 
 
 def mod4(v):
@@ -52,7 +53,7 @@
 def kernel(
     tok_h, gain_h, wg_h, wu_h, wd_h, ogain_h, out,
     tok, gain, wg, wu, wd, ogain, xg, xz, wb, wdb, part, zr, zs, rbuf, rdir, hall, hz, begun, psend, p1, p2, s1, s2, p3, p4,
-    sq_s, sq_r, sq2_r, sq3_r, st2_s, st_s, st_r, st_all, sq_n,
+    sq_s, sq_r, sq2_r, sq3_r, st2_s, st_all, sq_n,
     sent, head, loc, xa_rs, xb_rs, xc_rs, xz_rs, w_rs, f_rs, d_rs, df_rs, relay_rs, sum_rs, h_rs, hy_rs,
     p_rs, q_rs, t_rs, o_rs, of_rs,
 ):
@@ -324,46 +325,44 @@
         a, b = slice(r0, mid), slice(mid, r1)
         with scope(f"wait_p3#i={i}"):
             arrived(p3.at[:, a], p_rs.at[i, 2])
-        v = s1[x, a].astype(F32)
+        v1 = s1[x, a].astype(F32)
         for d in range(3):
-            v = v + p3[d, a].astype(F32)
-        pieces.append(v)
+            v1 = v1 + p3[d, a].astype(F32)
         with scope(f"wait_p4#i={i}"):
             arrived(p4.at[:, b], p_rs.at[i, 3])
-        v = s2[y, b].astype(F32)
+        v2 = s2[y, b].astype(F32)
         for d in range(3):
-            v = v + p4[d, b].astype(F32)
-        pieces.append(v)
-    piece = rows(c * H + x * B, B)
-    stream = 0.5 * tok[piece, :].astype(F32) + jnp.concatenate(pieces, axis=0)
-    out[piece, :] = stream.astype(BF16)
-
-    st_s[...] = row_sums(stream)
+            v2 = v2 + p4[d, b].astype(F32)
+        piece = rows(c * H + x * B + r0, r1 - r0)
+        pieces.append(0.5 * tok[piece, :].astype(F32) + jnp.concatenate([v1, v2], axis=0))
+        out[piece, :] = pieces[i].astype(BF16)
+        if i == 0:
+            for d in NEAR:
+                send(out.at[piece, :], out.at[piece, :], o_rs.at[i, d - 1], dev(dx=d))
+    stream = jnp.concatenate(pieces, axis=0)
+    mine = 2 * x + c
+    st_all[mine, 0] = row_sums(stream)
+    for dz, f, d, e in EVERYONE:
+        send(st_all.at[mine, 0], st_all.at[mine, 4 * dz + f], t_rs, dev(dz=dz, dy=f, dx=d, dc=e))
     for d in NEAR:
-        send(st_s, st_r.at[d - 1], t_rs.at[0], dev(dz=d))
-    ag = {d: send(out.at[piece, :], out.at[piece, :], o_rs.at[d - 1], dev(dx=d)) for d in NEAR}
-    with scope("wait_st"):
-        arrived(st_r, t_rs.at[0])
-    mine = 2 * x + c
-    st_all[mine, 0] = st_s[...] + st_r[0] + st_r[1] + st_r[2]
-    for f, d, e in PLANE:
-        send(st_all.at[mine, 0], st_all.at[mine, f], t_rs.at[1], dev(dy=f, dx=d, dc=e))
-    with scope("wait_o"):
-        for d in (0,) + NEAR:
-            if d:
-                ag[d].wait_recv()
-            block = out.at[rows(c * H + mod4(x - d) * B, B), :]
-            send(block, block, of_rs, dev(dc=1))
+        send(out.at[piece, :], out.at[piece, :], o_rs.at[1, d - 1], dev(dx=d))
+    for i, (r0, r1) in enumerate(HALVES):
+        with scope(f"wait_o#i={i}"):
+            for d in (0, 1, 3, 2):
+                block = out.at[rows(c * H + mod4(x - d) * B + r0, r1 - r0), :]
+                if d:
+                    arrived(block, o_rs.at[i, d - 1])
+                send(block, block, of_rs, dev(dc=1))
     with scope("wait_of"):
         arrived(out.at[:H], of_rs)
     with scope("wait_st2"):
-        arrived(sq_n.at[: len(PLANE)], t_rs.at[1])
+        arrived(sq_n.at[: len(EVERYONE)], t_rs)
     with scope("wait_sends"):
         for s in sends:
             s.wait_send()
     for xx in range(4):
         for cc in range(2):
-            total = st_all[2 * xx + cc, 0] + st_all[2 * xx + cc, 1] + st_all[2 * xx + cc, 2] + st_all[2 * xx + cc, 3]
+            total = jnp.sum(st_all[2 * xx + cc], axis=0)
             factor = as_columns(lax.rsqrt(total / D + EPS))
             r = slice(cc * H + xx * B, cc * H + (xx + 1) * B)
             for h in range(2):
@@ -418,10 +417,8 @@
             pltpu.VMEM((3, 1, L), F32),
             pltpu.VMEM((3, 1, L), F32),
             pltpu.VMEM((4, 1, L), F32),
-            pltpu.VMEM((1, L), F32),
-            pltpu.VMEM((3, 1, L), F32),
-            pltpu.VMEM((8, 4, 1, L), F32),
-            pltpu.VMEM((32, 1, L), F32),
+            pltpu.VMEM((8, 16, 1, L), F32),
+            pltpu.VMEM((128, 1, L), F32),
             dma,
             dma((6,)),
             dma((K + 1,)),
@@ -429,8 +426,8 @@
             dma((K, 3)), dma((K,)), dma((3,)), dma,
             dma((len(JOBS), 2)), dma((len(JOBS),)),
             dma((2,)), dma((2,)),
-            dma((2, 4)), dma((3,)), dma((2,)),
-            dma((3,)), dma,
+            dma((2, 4)), dma((3,)), dma,
+            dma((2, 3)), dma,
         ],
         compiler_params=pltpu.CompilerParams(
             collective_id=0, has_side_effects=True, vmem_limit_bytes=40 * 1024 * 1024

time: 66.6 us -> 65.1 us (0.977)
  Pallas kernels: 65.7 us -> 64.2 us
    pallas_call x1, Pallas kernels: 65.7 us -> 64.2 us  [body(): pl.pallas_call(kernel, out_shape=jax.ShapeDtypeStruct((T, W), BF16), in_s...]
where the time goes in v6:
time: 65.1 us; the launch traced here: 65 us
  Pallas kernels  64.2 us (99%)
  local copies, waits for them, and re-layouts  0.8 us (1%)
    pallas_call x1, Pallas kernels, body(): pl.pallas_call(kernel, out_shape=jax.ShapeDtypeStruct((T, W), BF16), in_s...  64.2 us

profile of v6, /device:TPU:1, one launch (start us, length us, event | category | flops | bytes accessed | tf_op | source)
XLA Modules:
  0.0 65.0 jit_solution(6183120067966542435)
XLA Ops:
  0.0 64.2 %shard_map.64 = bf16[1024,256]{1,0:T(8,128)(2,1)S(1)} custom-call(bf16[1024,256]{1,0:T(8,128)(2,1)} %tok_h.1, f32[1,256]{1,0:T(1,128)} %bitcast.4, bf16[256,1408]{1,0:T(8,128)(2,1)} %wg_h.1, bf16[256,1408]{1,0:T(8,128)(2,1)} %wu_h.1, bf16[11,128,256]{2,1,0:T(8,128)(2,1)} %bitcast.3, f32[1,256]{1,0:T(1,128)} %bitcast.5), custom_call_target="tpu_custom_call" | custom-call | tf_op jit(solution)/shard_map/pallas_call | solution.py:384
  64.2 0.8 %copy.8 = bf16[1024,256]{1,0:T(8,128)(2,1)} copy(bf16[1024,256]{1,0:T(8,128)(2,1)S(1)} %shard_map.64) | data formatting | bytes 1048576
